TPU v7x, 128 devices: a whole 4x4x4 slice. The times are simulated.
128 devices in a mesh: sp: 32 (over z, y, core), tp: 4 (over x).
Axes of the slice: x: 4, y: 4, z: 4, core: 2. Of those that a mesh axis runs over, the one named last changes fastest.
Arguments:
- tokens: bfloat16 [12288, 2048], P(('sp', 'tp')), may hold values from -8 to 8, as said below
- query_weight: bfloat16 [2048, 1024], P(None, 'tp'), as said below
- key_weight: bfloat16 [2048, 256], P(None, 'tp'), as said below
- value_weight: bfloat16 [2048, 256], P(None, 'tp'), may hold values from -0.125 to 0.125
- out_weight: bfloat16 [1024, 2048], P('tp'), may hold values from -0.75 to 0.75
- query_gain: bfloat16 [16, 64], P('tp'), may hold values from 0.5 to 6.5
- key_gain: bfloat16 [4, 64], P('tp'), may hold values from 0.5 to 6.5
Outputs:
- mixed: bfloat16 [12288, 2048], P(('sp', 'tp'))
- log_sums: float32 [16, 12288], P('tp', 'sp')
Inputs may be any that keep to these rules, and one draw needn't show every extreme that they name: Each block of 384 consecutive tokens has a mean vector of its own. `query_weight`: entries are those of a weight over 2048 inputs, of magnitude at most 6 / sqrt(2048). `key_weight`: entries are those of a weight over 2048 inputs, of magnitude at most 6 / sqrt(2048).
All inputs are finite; a program needn't handle non-finite values.
Results may differ from a plain program's by a relative error of at most 0.028.
Values may be sent and summed in bfloat16 or wider, within the bound.
A program may use at most 64 MiB of HBM per device.

v0:
```python
import functools
import math

import jax
import jax.numpy as jnp
from jax import lax
from jax.experimental import pallas as pl
from jax.experimental.pallas import tpu as pltpu
from jax.sharding import PartitionSpec as P

GRID_W = 64
ROPE_BASE = 10000.0
EPS = 1e-06
LOG2E = math.log2(math.e)
LN2 = math.log(2.0)
ONES = 16
MESH = pl.DeviceIdType.MESH
F32 = jnp.float32
BF16 = jnp.bfloat16


def prepare(x, gain, tables):
    quarter = x.shape[0] // 4
    x = x * lax.rsqrt(jnp.mean(x * x, axis=0, keepdims=True) + EPS) * gain
    a, b, c, d = (x[i * quarter : (i + 1) * quarter] for i in range(4))
    row_cos, row_sin, col_cos, col_sin = tables
    return jnp.concatenate(
        [
            a * row_cos - b * row_sin,
            b * row_cos + a * row_sin,
            c * col_cos - d * col_sin,
            d * col_cos + c * col_sin,
        ],
        axis=0,
    )


def angle_tables(first, count, quarter):
    place = first + lax.broadcasted_iota(jnp.int32, (quarter, count), 1)
    order = lax.broadcasted_iota(jnp.int32, (quarter, count), 0).astype(F32)
    freq = jnp.exp(order * (-math.log(ROPE_BASE) / quarter))
    shift = GRID_W.bit_length() - 1
    row = lax.shift_right_logical(place, shift).astype(F32) * freq
    col = jnp.bitwise_and(place, GRID_W - 1).astype(F32) * freq
    return (jnp.cos(row), jnp.sin(row), jnp.cos(col), jnp.sin(col))


def kernel(
    n_sp,
    n_tp,
    chunks,
    tok_hbm,
    wq_hbm,
    wk_hbm,
    wv_hbm,
    wo_hbm,
    qg_ref,
    kg_ref,
    mixed_ref,
    log_ref,
    tok,
    wq,
    wkv,
    wo,
    gains,
    raw,
    queries,
    kv,
    top,
    acc,
    att_own,
    att_out,
    att_in,
    part_out,
    part_in,
    local_sem,
    tok_send,
    tok_recv,
    wo_send,
    wo_recv,
    kv_send,
    kv_recv,
    att_send,
    att_recv,
    part_send,
    part_recv,
):
    sp = lax.axis_index("sp")
    tp = lax.axis_index("tp")
    pairs = n_tp // 2
    cols = n_sp // 2
    pair, core = tp // 2, tp % 2
    mate = pair * 2 + (1 - core)
    col, side = sp // 2, sp % 2
    other = col * 2 + (1 - side)
    rows = tok.shape[1]
    heads, width = qg_ref.shape
    kv_heads = kg_ref.shape[0]
    share = heads // kv_heads
    count = rows * n_tp

    def across(i):
        return lax.rem(pair + i, pairs) * 2 + core

    kv_cols = wk_hbm.shape[0]
    loads = [
        pltpu.make_async_copy(src, dst, local_sem.at[i])
        for i, (src, dst) in enumerate(
            ((tok_hbm, tok.at[tp]), (wq_hbm, wq), (wk_hbm, wkv.at[0:kv_cols]), (wv_hbm, wkv.at[kv_cols:]), (wo_hbm, wo.at[core]))
        )
    ]
    for load in loads:
        load.start()

    barrier = pltpu.get_barrier_semaphore()
    peers = 0
    for i in range(1, pairs):
        pl.semaphore_signal(barrier, inc=1, device_id={"tp": across(i)}, device_id_type=MESH)
        peers += 1
    pl.semaphore_signal(barrier, inc=1, device_id={"tp": mate}, device_id_type=MESH)
    pl.semaphore_signal(barrier, inc=1, device_id={"sp": other}, device_id_type=MESH)
    peers += 2
    for i in range(1, cols):
        peer = lax.rem(col + i, cols) * 2 + side
        pl.semaphore_signal(barrier, inc=1, device_id={"sp": peer}, device_id_type=MESH)
        peers += 1
    pl.semaphore_wait(barrier, peers)

    def send(src, dst, send_sem, recv_sem, where):
        return pltpu.make_async_remote_copy(
            src_ref=src,
            dst_ref=dst,
            send_sem=send_sem,
            recv_sem=recv_sem,
            device_id=where,
            device_id_type=MESH,
        )

    pending = []

    def go(copy):
        copy.start()
        pending.append(copy)

    def token_copy(block, src, slot, target):
        return send(src, tok.at[block], tok_send.at[slot], tok_recv.at[block], {"tp": target})

    for i in range(1, pairs):
        go(token_copy(tp, tok_hbm, i, across(i)))
    go(token_copy(tp, tok_hbm, 0, mate))

    gains[...] = jnp.zeros_like(gains)
    gains[0:heads, 0:width] = qg_ref[...].astype(F32) * (LOG2E * width ** (-0.5))
    gains[heads : heads + kv_heads, 0:width] = kg_ref[...].astype(F32)
    turned_gains = jnp.transpose(gains[...])
    tables = angle_tables(sp * count, count, width // 4)
    top[...] = jnp.full_like(top, -1e30)
    acc[...] = jnp.zeros_like(acc)
    loads[2].wait()
    loads[3].wait()
    loads[1].wait()
    loads[0].wait()
    query_cols = wq.shape[1]

    def project(block):
        piece = tok[block]
        at = pl.ds(pl.multiple_of(block * rows, rows), rows)
        raw[at, 0:query_cols] = jnp.dot(piece, wq[...], preferred_element_type=F32)
        raw[at, query_cols:] = lax.dot_general(
            piece, wkv[...], (((1,), (1,)), ((), ())), preferred_element_type=F32
        )

    kv_rows = kv_heads * width
    span = 2 * rows

    def span_of(part):
        return pl.ds(pl.multiple_of(part * span, span), span)

    def make_kv(part):
        at = span_of(part)
        turned = jnp.transpose(raw[at, query_cols : query_cols + kv_rows])
        angles = angle_tables(sp * count + part * span, span, width // 4)
        for h in range(kv_heads):
            gain = turned_gains[0:width, heads + h : heads + h + 1]
            keys = prepare(turned[h * width : (h + 1) * width], gain, angles)
            kv[sp, at, h * width : (h + 1) * width] = jnp.transpose(keys).astype(BF16)
        kv[sp, at, kv_rows : 2 * kv_rows] = raw[at, query_cols + kv_rows :].astype(BF16)

    def kv_copy(block, part, slot, where):
        spot = kv.at[block, span_of(part)]
        return send(spot, spot, kv_send.at[slot, part], kv_recv.at[block, part], {"sp": where})

    def near(distance, act):
        for way in (1, -1):
            place = col + distance * way

            @pl.when(jnp.logical_and(place >= 0, place < cols))
            def _():
                act(place)

    def to_column(place, part):
        return kv_copy(sp, part, place, place * 2 + side)

    def to_other(place, part):
        return kv_copy(place * 2 + side, part, cols + place, other)

    def send_kv(part):
        to_other(col, part).start()
        for distance in range(1, cols):
            near(distance, lambda place: to_column(place, part).start())

    def forward(place, part):
        kv_copy(place * 2 + side, part, 0, other).wait_recv()
        to_other(place, part).start()

    project(tp)
    token_copy(mate, tok_hbm, 0, mate).wait_recv()
    project(mate)
    make_kv(pair)
    send_kv(pair)
    for i in range(1, pairs):
        block = across(i)
        token_copy(block, tok_hbm, i, block).wait_recv()
        go(token_copy(block, tok.at[block], pairs + i, mate))
        project(block)
    loads[4].wait()
    wo_copy = send(wo_hbm, wo.at[core], wo_send, wo_recv, {"tp": mate})
    wo_copy.start()
    for i in range(1, pairs):
        block = lax.rem(pair + i, pairs) * 2 + (1 - core)
        token_copy(block, tok_hbm, i, mate).wait_recv()
        project(block)
        part = lax.rem(pair + i, pairs)
        make_kv(part)
        send_kv(part)
    for distance in range(1, cols):
        near(distance, lambda place: forward(place, pair))

    turned = jnp.transpose(raw[:, 0:query_cols])
    for h in range(heads):
        q = prepare(turned[h * width : (h + 1) * width], turned_gains[0:width, h : h + 1], tables)
        queries[h] = q.astype(BF16)

    def attend(block):
        ones = jnp.ones((ONES, count), BF16)
        turned = jnp.transpose(kv[block])
        for g in range(kv_heads):
            keys = kv[block, :, g * width : (g + 1) * width]
            values = turned[kv_rows + g * width : kv_rows + (g + 1) * width]
            values = jnp.concatenate([values, ones], axis=0)
            for h in range(g * share, (g + 1) * share):
                scores = jnp.dot(keys, queries[h], preferred_element_type=F32)
                old = top[h : h + 1, :]
                new = jnp.maximum(old, jnp.max(scores, axis=0, keepdims=True))
                weights = jnp.exp2(scores - new).astype(BF16)
                mixed = jnp.dot(values, weights, preferred_element_type=F32)
                acc[h] = acc[h] * jnp.exp2(old - new) + mixed
                top[h : h + 1, :] = new

    def straight(place):
        for i in range(1, pairs):
            forward(place, lax.rem(pair + i, pairs))
        attend(place * 2 + side)

    def mirrored(place):
        block = place * 2 + (1 - side)
        for part in range(pairs):
            kv_copy(block, part, 0, other).wait_recv()
        attend(block)

    attend(sp)
    mirrored(col)

    def step(distance, carry):
        near(distance, straight)

        @pl.when(distance > 1)
        def _():
            near(distance - 1, mirrored)

        return carry

    lax.fori_loop(1, cols, step, 0)
    near(cols - 1, mirrored)

    finished = []
    for h in range(heads):
        total = acc[h, width : width + 1, :]
        finished.append(acc[h, 0:width, :] / total)
        log_ref[h : h + 1, :] = (top[h : h + 1, :] + jnp.log2(total)) * LN2
    attended = jnp.transpose(jnp.concatenate(finished, axis=0)).astype(BF16)
    for t in range(n_tp):
        piece = attended[t * rows : (t + 1) * rows]

        @pl.when(core == t % 2)
        def _():
            att_own[t // 2] = piece

        @pl.when(core != t % 2)
        def _():
            att_out[t // 2] = piece

    att_copy = send(att_out, att_in, att_send, att_recv, {"tp": mate})
    att_copy.start()
    att_copy.wait_recv()
    wo_copy.wait_recv()
    step_cols = mixed_ref.shape[1] // chunks

    def product(place, n):
        at = slice(n * step_cols, (n + 1) * step_cols)
        return jnp.dot(
            att_own[place], wo[core, :, at], preferred_element_type=F32
        ) + jnp.dot(att_in[place], wo[1 - core, :, at], preferred_element_type=F32)

    def part_copy(i, n):
        slot = (i - 1) * chunks + n
        return send(
            part_out.at[slot],
            part_in.at[slot],
            part_send.at[slot],
            part_recv.at[slot],
            {"tp": across(i)},
        )

    for n in range(chunks):
        for i in range(1, pairs):
            part_out[(i - 1) * chunks + n] = product(lax.rem(pair + i, pairs), n).astype(BF16)
            part_copy(i, n).start()
    for n in range(chunks):
        at = slice(n * step_cols, (n + 1) * step_cols)
        total = product(pair, n)
        for i in range(1, pairs):
            part_copy(i, n).wait_recv()
            total = total + part_in[(i - 1) * chunks + n].astype(F32)
        mixed_ref[:, at] = total.astype(BF16)

    for copy in pending:
        copy.wait_send()
    wo_copy.wait_send()
    att_copy.wait_send()
    for part in range(pairs):
        to_other(col, part).wait_send()
        for distance in range(1, cols):
            near(distance, lambda place: to_column(place, part).wait_send())
            near(distance, lambda place: to_other(place, part).wait_send())
    for n in range(chunks):
        for i in range(1, pairs):
            part_copy(i, n).wait_send()


def body(n_sp, n_tp, tokens, query_weight, key_weight, value_weight, out_weight, query_gain, key_gain):
    rows, depth = tokens.shape
    query_cols = query_weight.shape[1]
    kv_cols = key_weight.shape[1]
    heads, width = query_gain.shape
    kv_heads = key_gain.shape[0]
    group, model = out_weight.shape
    count = rows * n_tp
    pairs, cols = n_tp // 2, n_sp // 2
    chunks = 4
    any_space = pl.BlockSpec(memory_space=pl.ANY)
    vmem = pl.BlockSpec(memory_space=pltpu.VMEM)
    dma = pltpu.SemaphoreType.DMA
    slots = max(pairs - 1, 1) * chunks
    return pl.pallas_call(
        functools.partial(kernel, n_sp, n_tp, chunks),
        out_shape=(
            pltpu.VMEM((rows, model), BF16),
            pltpu.VMEM((heads, count), F32),
        ),
        in_specs=[any_space] * 5 + [vmem] * 2,
        out_specs=(vmem, vmem),
        scratch_shapes=[
            pltpu.VMEM((n_tp, rows, depth), BF16),
            pltpu.VMEM((depth, query_cols), BF16),
            pltpu.VMEM((2 * kv_cols, depth), BF16),
            pltpu.VMEM((2, group, model), BF16),
            pltpu.VMEM((128, 128), F32),
            pltpu.VMEM((count, query_cols + 2 * kv_cols), F32),
            pltpu.VMEM((heads, width, count), BF16),
            pltpu.VMEM((n_sp, count, 2 * kv_heads * width), BF16),
            pltpu.VMEM((heads, count), F32),
            pltpu.VMEM((heads, width + ONES, count), F32),
            pltpu.VMEM((pairs, rows, group), BF16),
            pltpu.VMEM((pairs, rows, group), BF16),
            pltpu.VMEM((pairs, rows, group), BF16),
            pltpu.VMEM((slots, rows, model // chunks), BF16),
            pltpu.VMEM((slots, rows, model // chunks), BF16),
            dma((5,)),
            dma((2 * pairs,)),
            dma((n_tp,)),
            dma,
            dma,
            dma((2 * cols, pairs)),
            dma((n_sp, pairs)),
            dma,
            dma,
            dma((slots,)),
            dma((slots,)),
        ],
        compiler_params=pltpu.CompilerParams(
            collective_id=0, has_side_effects=True, vmem_limit_bytes=60 * 1024 * 1024
        ),
        name="attention",
    )(tokens, query_weight, key_weight.T, value_weight.T, out_weight, query_gain, key_gain)


def solution(mesh):
    return jax.shard_map(
        functools.partial(body, mesh.shape["sp"], mesh.shape["tp"]),
        mesh=mesh,
        in_specs=(
            P(("sp", "tp"), None),
            P(None, "tp"),
            P(None, "tp"),
            P(None, "tp"),
            P("tp", None),
            P("tp", None),
            P("tp", None),
        ),
        out_specs=(P(("sp", "tp"), None), P("tp", "sp")),
        check_vma=False,
    )
```

profile of v0, /device:TPU:1, one launch (start us, length us, event | category | flops | bytes accessed | tf_op | source)
XLA Modules:
  0.0 108.0 jit_solution(1461060815429418211)
XLA Ops:
  0.6 106.0 %attention.1 = (bf16[96,2048]{1,0:T(8,128)(2,1)S(1)}, f32[4,384]{1,0:T(4,128)S(1)}) custom-call(bf16[96,2048]{1,0:T(8,128)(2,1)} %tok_hbm.1, bf16[2048,256]{1,0:T(8,128)(2,1)} %wq_hbm.1, bf16[64,2048]{1,0:T(8,128)(2,1)} %bitcast.2, bf16[64,2048]{1,0:T(8,128)(2,1)} %bitcast.3, bf16[256,2048]{1,0:T(8,128)(2,1)} %wo_hbm.1, bf16[4,64]{1,0:T(4,128)(2,1)} %qg_ref.1, ...), custom_call_target="tpu_custom_call" | custom-call | tf_op jit(solution)/shard_map/attention/pallas_call | solution.py:365
  106.6 0.7 copy.11
  107.4 0.6 copy.12
where the time goes:
time: 110 us; the launch traced here: 108 us
  Pallas kernels  106 us (96%)
  local copies, waits for them, and re-layouts  1.34 us (1%)
    pallas_call x1, Pallas kernels, body(): pl.pallas_call(functools.partial(kernel, n_sp, n_tp, chunks), out_shape=(...  106 us

commit v1 on v0

v1 whole, which is shorter than its diff:
```python
import functools
import math

import jax
import jax.numpy as jnp
from jax import lax
from jax.experimental import pallas as pl
from jax.experimental.pallas import tpu as pltpu
from jax.sharding import PartitionSpec as P

GRID_W = 64
ROPE_BASE = 10000.0
EPS = 1e-06
LOG2E = math.log2(math.e)
LN2 = math.log(2.0)
ONES = 16
RING = 4
CHUNK = 768
TILE = 256
SUB = 256
MESH = pl.DeviceIdType.MESH
F32 = jnp.float32
BF16 = jnp.bfloat16


def prepare(x, gain, tables):
    quarter = x.shape[0] // 4
    x = x * lax.rsqrt(jnp.mean(x * x, axis=0, keepdims=True) + EPS) * gain
    a, b, c, d = (x[i * quarter : (i + 1) * quarter] for i in range(4))
    row_cos, row_sin, col_cos, col_sin = tables
    return jnp.concatenate(
        [
            a * row_cos - b * row_sin,
            b * row_cos + a * row_sin,
            c * col_cos - d * col_sin,
            d * col_cos + c * col_sin,
        ],
        axis=0,
    )


def angle_tables(first, count, quarter):
    place = first + lax.broadcasted_iota(jnp.int32, (quarter, count), 1)
    order = lax.broadcasted_iota(jnp.int32, (quarter, count), 0).astype(F32)
    freq = jnp.exp(order * (-math.log(ROPE_BASE) / quarter))
    shift = GRID_W.bit_length() - 1
    row = lax.shift_right_logical(place, shift).astype(F32) * freq
    col = jnp.bitwise_and(place, GRID_W - 1).astype(F32) * freq
    return (jnp.cos(row), jnp.sin(row), jnp.cos(col), jnp.sin(col))


def kernel(
    tok_hbm,
    wq_hbm,
    wk_hbm,
    wv_hbm,
    wo_hbm,
    qg_ref,
    kg_ref,
    mixed_ref,
    log_ref,
    tok,
    wq,
    wkv,
    wo,
    gains,
    raw,
    queries,
    kv,
    scores,
    peak,
    turned_v,
    acc,
    top,
    att,
    att_in,
    local_sem,
    tok_send,
    tok_recv,
    kv_send,
    kv_recv,
    wo_send,
    wo_recv,
    att_send,
    att_recv,
):
    sp = lax.axis_index("sp")
    tp = lax.axis_index("tp")
    core = lax.rem(sp, 2)
    y = lax.rem(sp // 2, RING)
    z = sp // (2 * RING)
    mate = sp + 1 - 2 * core
    left, right, opposite = (lax.rem(tp + i, RING) for i in (3, 1, 2))
    n_sp = RING * RING * 2
    rows = tok.shape[1]
    half = rows // 2
    heads, width = qg_ref.shape
    count = rows * RING
    query_cols = wq.shape[1]
    kv_cols = wk_hbm.shape[0]
    group = wo_hbm.shape[0]
    n_tiles = heads * count // TILE
    n_chunks = n_sp * count // CHUNK

    coord_a = y * (1 - core) + z * core
    step_a = 2 + 6 * core
    coord_b = z * (1 - core) + y * core
    step_b = 8 - 6 * core

    def shift_a(i):
        return (lax.rem(coord_a + i, RING) - coord_a) * step_a

    def shift_b(i):
        return (lax.rem(coord_b + i, RING) - coord_b) * step_b

    loads = [
        pltpu.make_async_copy(src, dst, local_sem.at[i])
        for i, (src, dst) in enumerate(
            (
                (tok_hbm, tok.at[tp]),
                (wq_hbm, wq),
                (wk_hbm, wkv.at[0:kv_cols]),
                (wv_hbm, wkv.at[kv_cols:]),
                (wo_hbm, wo.at[tp]),
            )
        )
    ]
    for load in loads:
        load.start()

    barrier = pltpu.get_barrier_semaphore()
    for i in range(1, RING):
        pl.semaphore_signal(barrier, inc=1, device_id={"tp": lax.rem(tp + i, RING)}, device_id_type=MESH)
        pl.semaphore_signal(barrier, inc=1, device_id={"sp": sp + shift_a(i)}, device_id_type=MESH)
        pl.semaphore_signal(barrier, inc=1, device_id={"sp": sp + shift_b(i)}, device_id_type=MESH)
    pl.semaphore_signal(barrier, inc=1, device_id={"sp": mate}, device_id_type=MESH)
    pl.semaphore_wait(barrier, 3 * (RING - 1) + 1)

    pending = []

    def send(src, dst, send_sem, recv_sem, where):
        return pltpu.make_async_remote_copy(
            src_ref=src,
            dst_ref=dst,
            send_sem=send_sem,
            recv_sem=recv_sem,
            device_id=where,
            device_id_type=MESH,
        )

    def go(copy):
        copy.start()
        pending.append(copy)

    def part(i):
        return slice(i * half, (i + 1) * half)

    def token_copy(block, i, slot, where, src=None):
        src = tok.at[block, part(i)] if src is None else src
        return send(src, tok.at[block, part(i)], tok_send.at[slot], tok_recv.at[block, i], {"tp": where})

    go(token_copy(tp, 0, 0, right, tok_hbm.at[part(0)]))
    go(token_copy(tp, 1, 1, left, tok_hbm.at[part(1)]))
    go(token_copy(tp, 1, 2, right, tok_hbm.at[part(1)]))
    go(token_copy(tp, 0, 3, left, tok_hbm.at[part(0)]))

    gains[...] = jnp.zeros_like(gains)
    gains[0:heads, 0:width] = qg_ref[...].astype(F32) * (LOG2E * width ** (-0.5))
    gains[heads : heads + 1, 0:width] = kg_ref[...].astype(F32)
    turned_gains = jnp.transpose(gains[...])
    top[...] = jnp.full_like(top, -1e30)
    acc[...] = jnp.zeros_like(acc)
    turned_v[:, width:, :] = jnp.ones_like(turned_v[:, width:, :])

    def project(block):
        piece = tok[block]
        at = pl.ds(pl.multiple_of(block * rows, rows), rows)
        raw[at, 0:query_cols] = jnp.dot(piece, wq[...], preferred_element_type=F32)
        raw[at, query_cols:] = lax.dot_general(
            piece, wkv[...], (((1,), (1,)), ((), ())), preferred_element_type=F32
        )

    sizes = (rows, 2 * rows, rows)
    bases = (0, n_sp * rows, 3 * n_sp * rows)

    def make_kv(block, p, offset):
        at = pl.ds(pl.multiple_of(block * rows, rows), rows)
        turned = jnp.transpose(raw[at, query_cols:])
        angles = angle_tables(sp * count + block * rows, rows, width // 4)
        keys = prepare(turned[0:width], turned_gains[0:width, heads : heads + 1], angles)
        to = pl.ds(pl.multiple_of(bases[p] + sp * sizes[p] + offset, rows), rows)
        kv[to, 0:width] = jnp.transpose(keys).astype(BF16)
        kv[to, width : 2 * width] = raw[at, query_cols + width :].astype(BF16)

    def kv_copy(block, p, slot, where):
        spot = kv.at[pl.ds(pl.multiple_of(bases[p] + block * sizes[p], rows), sizes[p])]
        return send(spot, spot, kv_send.at[p, slot], kv_recv.at[block, p], {"sp": where})

    def own_send(p):
        for i in range(1, RING):
            go(kv_copy(sp, p, i - 1, sp + shift_a(i)))
        for i in range(1, RING):
            go(kv_copy(sp, p, i + 2, sp + shift_b(i)))
        go(kv_copy(sp, p, 6, mate))

    def spread_copies(p):
        for k in range(1, RING):
            block = sp + shift_a(k)
            yield [
                kv_copy(block, p, 7 + (k - 1) * RING + j - 1, sp + shift_b(j)) for j in range(1, RING)
            ] + [kv_copy(block, p, 7 + (k - 1) * RING + RING - 1, mate)]

    def spread(p):
        for copies in spread_copies(p):
            copies[0].wait_recv()
            for copy in copies:
                copy.start()

    def hand_copies(p):
        for j in range(1, RING):
            for k in range(RING):
                yield kv_copy(sp + shift_a(k) + shift_b(j), p, 19 + (j - 1) * RING + k, mate)

    def hand(p):
        for copy in hand_copies(p):
            copy.wait_recv()
            copy.start()

    def from_mate(p):
        for chip in range(RING * RING):
            kv_copy(2 * chip + 1 - core, p, 0, mate).wait_recv()

    quarter = group // 4

    def wo_at(block, side, i):
        return wo.at[block, pl.ds(pl.multiple_of(side * 2 * quarter + i * quarter, quarter), quarter)]

    def wo_copy(block, side, i, slot, where):
        spot = wo_at(block, side, i)
        return send(spot, spot, wo_send.at[slot], wo_recv.at[block, side, i], where)

    def wo_first():
        return [
            wo_copy(tp, core, 0, 0, {"tp": right}),
            wo_copy(tp, core, 1, 1, {"tp": left}),
            wo_copy(tp, core, 1, 2, {"tp": right}),
            wo_copy(tp, core, 0, 3, {"tp": left}),
        ]

    def wo_forward():
        return [wo_copy(left, core, 0, 4, {"tp": right}), wo_copy(right, core, 1, 5, {"tp": left})]

    hand_order = ((left, 0), (right, 1), (left, 1), (right, 0), (opposite, 0), (opposite, 1))

    def wo_hand(n):
        block, i = hand_order[n]
        return wo_copy(block, core, i, 6 + n, {"sp": mate})

    loads[2].wait()
    loads[3].wait()
    loads[1].wait()
    loads[0].wait()
    project(tp)
    make_kv(tp, 0, 0)
    own_send(0)
    token_copy(left, 0, 0, right).wait_recv()
    go(token_copy(left, 0, 4, right))
    token_copy(right, 1, 0, left).wait_recv()
    go(token_copy(right, 1, 5, left))
    spread(0)
    token_copy(left, 1, 0, right).wait_recv()
    project(left)
    make_kv(left, 1, 0)
    token_copy(right, 0, 0, left).wait_recv()
    project(right)
    make_kv(right, 1, rows)
    own_send(1)
    hand(0)
    spread(1)
    loads[4].wait()
    token_copy(opposite, 0, 0, right).wait_recv()
    token_copy(opposite, 1, 0, left).wait_recv()
    for copy in wo_first():
        copy.start()
    project(opposite)
    make_kv(opposite, 2, 0)
    own_send(2)

    tables = angle_tables(sp * count, count, width // 4)
    turned = jnp.transpose(raw[:, 0:query_cols])
    for h in range(heads):
        q = prepare(turned[h * width : (h + 1) * width], turned_gains[0:width, h : h + 1], tables)
        queries[:, h * count : (h + 1) * count] = q.astype(BF16)
    from_mate(0)

    def turn(chunk, slot):
        at = pl.ds(pl.multiple_of(chunk * CHUNK, CHUNK), CHUNK)
        turned_v[slot, 0:width] = jnp.transpose(kv[at])[width : 2 * width]

    def score(chunk, t, slot, i):
        at = pl.ds(pl.multiple_of(chunk * CHUNK + i * SUB, SUB), SUB)
        s = jnp.dot(kv[at, 0:width], queries[:, t * TILE : (t + 1) * TILE], preferred_element_type=F32)
        scores[slot, i * SUB : (i + 1) * SUB] = s
        return jnp.max(s.reshape(SUB // 8, 8, TILE), axis=0)

    def score_all(chunk, t, slot):
        best = None
        for i in range(CHUNK // SUB):
            m = score(chunk, t, slot, i)
            best = m if best is None else jnp.maximum(best, m)
        peak[slot] = best

    turn(0, 0)
    score_all(0, 0, 0)
    score_all(0, 1, 1)

    def step(j, carry):
        @pl.when(j == 1)
        def _():
            spread(2)

        @pl.when(j == 2)
        def _():
            hand(1)

        @pl.when(j == 3)
        def _():
            from_mate(1)

        @pl.when(j == 6)
        def _():
            for copy, n in zip(wo_forward(), (0, 1)):
                copy.wait_recv()
                copy.start()
                wo_hand(n).start()
            hand(2)

        @pl.when(j == 11)
        def _():
            from_mate(2)

        @pl.when(j == 13)
        def _():
            for n in (2, 3):
                wo_hand(n).wait_recv()
                wo_hand(n).start()

        now = lax.rem(j, 2)
        later = lax.rem(j + 1, n_chunks)
        for t in range(n_tiles):
            if t == 1:
                turn(later, 1 - now)
            chunk, tile = (j, t + 2) if t + 2 < n_tiles else (later, t + 2 - n_tiles)
            fill, slot = (t + 2) % 3, t % 3
            old = top[t]
            new = jnp.maximum(old, jnp.max(peak[slot], axis=0, keepdims=True))
            best = None
            total = None
            for i in range(CHUNK // SUB):
                m = score(chunk, tile, fill, i)
                best = m if best is None else jnp.maximum(best, m)
                at = slice(i * SUB, (i + 1) * SUB)
                weights = jnp.exp2(scores[slot, at] - new).astype(BF16)
                mixed = jnp.dot(turned_v[now, :, at], weights, preferred_element_type=F32)
                total = mixed if total is None else total + mixed
            peak[fill] = best
            acc[t] = acc[t] * jnp.exp2(old - new) + total
            top[t] = new
        return carry

    lax.fori_loop(0, n_chunks, step, 0)

    for n in (4, 5):
        wo_hand(n).wait_recv()
        wo_hand(n).start()

    flat = [acc[t] for t in range(n_tiles)]
    sums = jnp.concatenate([f[width : width + 1] for f in flat], axis=1)
    outs = jnp.concatenate([f[0:width] / f[width : width + 1] for f in flat], axis=1)
    logs = (jnp.concatenate([top[t] for t in range(n_tiles)], axis=1) + jnp.log2(sums)) * LN2
    finished = []
    for h in range(heads):
        at = slice(h * count, (h + 1) * count)
        finished.append(outs[:, at])
        log_ref[h : h + 1, :] = logs[:, at]
    att[...] = jnp.transpose(jnp.concatenate(finished, axis=0)).astype(BF16)

    def att_copy(i):
        to = lax.rem(tp + i, RING)
        src = att.at[pl.ds(pl.multiple_of(to * rows, rows), rows)]
        return send(src, att_in.at[tp], att_send.at[i - 1], att_recv.at[tp], {"tp": to})

    for i in (2, 1, 3):
        att_copy(i).start()

    def att_wait(block):
        send(att_in.at[block], att_in.at[block], att_send.at[0], att_recv.at[block], {"tp": right}).wait_recv()

    for block, i in hand_order:
        wo_copy(block, 1 - core, i, 0, {"sp": mate}).wait_recv()
    own = att[pl.ds(pl.multiple_of(tp * rows, rows), rows)]
    for block in (left, right, opposite):
        att_wait(block)
    model = mixed_ref.shape[1]
    cols = 512
    for n in range(model // cols):
        at = slice(n * cols, (n + 1) * cols)
        total = jnp.dot(own, wo[tp, :, at], preferred_element_type=F32)
        for block in (left, right, opposite):
            total = total + jnp.dot(att_in[block], wo[block, :, at], preferred_element_type=F32)
        mixed_ref[:, at] = total.astype(BF16)

    for copy in pending:
        copy.wait_send()
    for p in (0, 1, 2):
        for copies in spread_copies(p):
            for copy in copies:
                copy.wait_send()
        for copy in hand_copies(p):
            copy.wait_send()
    for copy in wo_first() + wo_forward() + [wo_hand(n) for n in range(6)]:
        copy.wait_send()
    for i in range(1, RING):
        att_copy(i).wait_send()


def body(tokens, query_weight, key_weight, value_weight, out_weight, query_gain, key_gain):
    rows, depth = tokens.shape
    query_cols = query_weight.shape[1]
    kv_cols = key_weight.shape[1]
    heads, width = query_gain.shape
    group, model = out_weight.shape
    count = rows * RING
    n_sp = RING * RING * 2
    n_tiles = heads * count // TILE
    any_space = pl.BlockSpec(memory_space=pl.ANY)
    vmem = pl.BlockSpec(memory_space=pltpu.VMEM)
    dma = pltpu.SemaphoreType.DMA
    return pl.pallas_call(
        kernel,
        out_shape=(
            pltpu.VMEM((rows, model), BF16),
            pltpu.VMEM((heads, count), F32),
        ),
        in_specs=[any_space] * 5 + [vmem] * 2,
        out_specs=(vmem, vmem),
        scratch_shapes=[
            pltpu.VMEM((RING, rows, depth), BF16),
            pltpu.VMEM((depth, query_cols), BF16),
            pltpu.VMEM((2 * kv_cols, depth), BF16),
            pltpu.VMEM((RING, group, model), BF16),
            pltpu.VMEM((128, 128), F32),
            pltpu.VMEM((count, query_cols + 2 * kv_cols), F32),
            pltpu.VMEM((width, heads * count), BF16),
            pltpu.VMEM((n_sp * count, 2 * width), BF16),
            pltpu.VMEM((3, CHUNK, TILE), F32),
            pltpu.VMEM((3, 8, TILE), F32),
            pltpu.VMEM((2, width + ONES, CHUNK), BF16),
            pltpu.VMEM((n_tiles, width + ONES, TILE), F32),
            pltpu.VMEM((n_tiles, 1, TILE), F32),
            pltpu.VMEM((count, group), BF16),
            pltpu.VMEM((RING, rows, group), BF16),
            dma((5,)),
            dma((6,)),
            dma((RING, 2)),
            dma((3, 31)),
            dma((n_sp, 3)),
            dma((12,)),
            dma((RING, 2, 2)),
            dma((RING - 1,)),
            dma((RING,)),
        ],
        compiler_params=pltpu.CompilerParams(
            collective_id=0, has_side_effects=True, vmem_limit_bytes=60 * 1024 * 1024
        ),
        name="attention",
    )(tokens, query_weight, key_weight.T, value_weight.T, out_weight, query_gain, key_gain)


def solution(mesh):
    return jax.shard_map(
        body,
        mesh=mesh,
        in_specs=(
            P(("sp", "tp"), None),
            P(None, "tp"),
            P(None, "tp"),
            P(None, "tp"),
            P("tp", None),
            P("tp", None),
            P("tp", None),
        ),
        out_specs=(P(("sp", "tp"), None), P("tp", "sp")),
        check_vma=False,
    )
```

time: 110 us -> 59.3 us (0.54); the launches traced: 108 us -> 59.2 us
  Pallas kernels: 106 us -> 57.2 us
    pallas_call x1, Pallas kernels: 106 us -> 57.2 us  [body(): pl.pallas_call(kernel, out_shape=(pltpu.VMEM((rows, model), BF16), pltpu....]
where the time goes in v1:
time: 59.3 us; the launch traced here: 59.2 us
  Pallas kernels  57.2 us (96%)
  local copies, waits for them, and re-layouts  1.34 us (2%)
  between operations  0.64 us (1%)
    pallas_call x1, Pallas kernels, body(): pl.pallas_call(kernel, out_shape=(pltpu.VMEM((rows, model), BF16), pltpu....  57.2 us
    unnamed x2, local copies, waits for them, and re-layouts  1.34 us

profile of v1, /device:TPU:1, one launch (start us, length us, event | category | flops | bytes accessed | tf_op | source)
XLA Modules:
  0.0 59.2 jit_solution(413647523105852428)
XLA Ops:
  0.6 57.2 %attention.1 = (bf16[96,2048]{1,0:T(8,128)(2,1)S(1)}, f32[4,384]{1,0:T(4,128)S(1)}) custom-call(bf16[96,2048]{1,0:T(8,128)(2,1)} %tok_hbm.1, bf16[2048,256]{1,0:T(8,128)(2,1)} %wq_hbm.1, bf16[64,2048]{1,0:T(8,128)(2,1)} %bitcast.2, bf16[64,2048]{1,0:T(8,128)(2,1)} %bitcast.3, bf16[256,2048]{1,0:T(8,128)(2,1)} %wo_hbm.1, bf16[4,64]{1,0:T(4,128)(2,1)} %qg_ref.1, ...), custom_call_target="tpu_custom_call" | custom-call | tf_op jit(solution)/shard_map/attention/pallas_call | solution.py:439
  57.9 0.7 %copy.11 = bf16[96,2048]{1,0:T(8,128)(2,1)} copy(bf16[96,2048]{1,0:T(8,128)(2,1)S(1)} %get-tuple-element.2) | data formatting | bytes 786432
  58.6 0.6 %copy.12 = f32[4,384]{1,0:T(4,128)} copy(f32[4,384]{1,0:T(4,128)S(1)} %get-tuple-element.3) | data formatting | bytes 12288

commit v2 on v1

v2 whole, which is shorter than its diff:
```python
import functools
import math

import jax
import jax.numpy as jnp
from jax import lax
from jax.experimental import pallas as pl
from jax.experimental.pallas import tpu as pltpu
from jax.sharding import PartitionSpec as P

GRID_W = 64
ROPE_BASE = 10000.0
EPS = 1e-06
LOG2E = math.log2(math.e)
LN2 = math.log(2.0)
ONES = 16
RING = 4
CHUNK = 768
TILE = 256
SUB = 256
MESH = pl.DeviceIdType.MESH
F32 = jnp.float32
BF16 = jnp.bfloat16


def prepare(x, gain, tables):
    quarter = x.shape[0] // 4
    x = x * lax.rsqrt(jnp.mean(x * x, axis=0, keepdims=True) + EPS) * gain
    a, b, c, d = (x[i * quarter : (i + 1) * quarter] for i in range(4))
    row_cos, row_sin, col_cos, col_sin = tables
    return jnp.concatenate(
        [
            a * row_cos - b * row_sin,
            b * row_cos + a * row_sin,
            c * col_cos - d * col_sin,
            d * col_cos + c * col_sin,
        ],
        axis=0,
    )


def kernel(
    tok_hbm,
    wq_hbm,
    wk_hbm,
    wv_hbm,
    wo_hbm,
    qg_ref,
    kg_ref,
    mixed_ref,
    log_ref,
    tok,
    wq,
    wkv,
    wo,
    gain_cols,
    tables,
    queries,
    kv,
    scores,
    peak,
    turned_v,
    acc,
    top,
    att,
    att_in,
    log_rows,
    product,
    local_sem,
    tok_send,
    tok_recv,
    kv_send,
    kv_recv,
    wo_send,
    wo_recv,
    att_send,
    att_recv,
):
    sp = lax.axis_index("sp")
    tp = lax.axis_index("tp")
    core = lax.rem(sp, 2)
    y = lax.rem(sp // 2, RING)
    z = sp // (2 * RING)
    mate = sp + 1 - 2 * core
    left, right, opposite = (lax.rem(tp + i, RING) for i in (3, 1, 2))
    rows = tok.shape[1]
    half = rows // 2
    heads, width = qg_ref.shape
    count = rows * RING
    kv_cols = wk_hbm.shape[0]
    group, model = wo_hbm.shape
    n_tiles = 2 * heads * rows // TILE

    coord_a = y * (1 - core) + z * core
    step_a = 2 + 6 * core
    coord_b = z * (1 - core) + y * core
    step_b = 8 - 6 * core

    def peer_a(i):
        return {"sp": sp + (lax.rem(coord_a + i, RING) - coord_a) * step_a}

    def peer_b(i):
        return {"sp": sp + (lax.rem(coord_b + i, RING) - coord_b) * step_b}

    loads = [
        pltpu.make_async_copy(src, dst, local_sem.at[i])
        for i, (src, dst) in enumerate(
            (
                (tok_hbm, tok.at[0]),
                (wk_hbm, wkv.at[0:kv_cols]),
                (wv_hbm, wkv.at[kv_cols:]),
                (wq_hbm, wq),
                (wo_hbm, wo.at[0]),
            )
        )
    ]
    for load in loads:
        load.start()

    barrier = pltpu.get_barrier_semaphore()
    for i in range(1, RING):
        pl.semaphore_signal(barrier, inc=1, device_id={"tp": lax.rem(tp + i, RING)}, device_id_type=MESH)
        pl.semaphore_signal(barrier, inc=1, device_id=peer_a(i), device_id_type=MESH)
        pl.semaphore_signal(barrier, inc=1, device_id=peer_b(i), device_id_type=MESH)
    pl.semaphore_signal(barrier, inc=1, device_id={"sp": mate}, device_id_type=MESH)
    pl.semaphore_wait(barrier, 3 * (RING - 1) + 1)

    def send(src, dst, send_sem, recv_sem, where):
        return pltpu.make_async_remote_copy(
            src_ref=src,
            dst_ref=dst,
            send_sem=send_sem,
            recv_sem=recv_sem,
            device_id=where,
            device_id_type=MESH,
        )

    def part(i):
        return slice(i * half, (i + 1) * half)

    to_left, to_right, to_opposite, to_mate = {"tp": left}, {"tp": right}, {"tp": opposite}, {"sp": mate}

    def token_copy(src, piece, i, slot, where):
        return send(src, tok.at[piece, part(i)], tok_send.at[slot], tok_recv.at[piece, i], where)

    first_half, second_half = tok_hbm.at[part(0)], tok_hbm.at[part(1)]
    token_out = [
        token_copy(first_half, 1, 0, 0, to_right),
        token_copy(second_half, 1, 1, 1, to_left),
        token_copy(second_half, 2, 0, 2, to_right),
        token_copy(first_half, 2, 1, 3, to_left),
    ]
    token_on = [
        token_copy(tok.at[1, part(0)], 3, 0, 4, to_right),
        token_copy(tok.at[1, part(1)], 3, 1, 5, to_left),
    ]
    for copy in token_out:
        copy.start()

    def token_wait(piece, i):
        token_copy(tok.at[1, part(i)], piece, i, 4 + i, to_right).wait_recv()

    starts = (
        (tp * rows, tp * rows + half),
        (left * rows, right * rows + half),
        (left * rows + half, right * rows),
        (opposite * rows, opposite * rows + half),
    )

    quarter = width // 4
    lane = lax.broadcasted_iota(jnp.int32, (quarter, heads * rows), 1)
    spot = lane
    for h in range(1, heads):
        spot = spot - jnp.where(lane >= h * rows, rows, 0)
    order = lax.broadcasted_iota(jnp.int32, (quarter, heads * rows), 0).astype(F32)
    freq = jnp.exp(order * (-math.log(ROPE_BASE) / quarter))
    shift = GRID_W.bit_length() - 1
    for p in range(4):
        a, b = starts[p]
        place = sp * count + spot + jnp.where(spot < half, a, b - half)
        row = lax.shift_right_logical(place, shift).astype(F32) * freq
        col = jnp.bitwise_and(place, GRID_W - 1).astype(F32) * freq
        tables[p, 0:quarter] = jnp.cos(row)
        tables[p, quarter : 2 * quarter] = jnp.sin(row)
        tables[p, 2 * quarter : 3 * quarter] = jnp.cos(col)
        tables[p, 3 * quarter :] = jnp.sin(col)

    gain_rows = [
        jnp.broadcast_to(qg_ref[h : h + 1, :].astype(F32) * (LOG2E * width ** (-0.5)), (rows, width))
        for h in range(heads)
    ]
    gain_rows.append(jnp.broadcast_to(kg_ref[...].astype(F32), (128, width)))
    gain_cols[...] = jnp.transpose(jnp.concatenate(gain_rows, axis=0))
    top[...] = jnp.full_like(top, -1e30)
    acc[...] = jnp.zeros_like(acc)
    turned_v[:, width:, :] = jnp.ones_like(turned_v[:, width:, :])
    log_rows[...] = jnp.zeros_like(log_rows)

    def kv_rows(p, j, c, k):
        return pl.ds(pl.multiple_of((((p * RING + j) * 2 + c) * RING + k) * rows, rows), rows)

    def tables_of(p, n):
        return [tables[p, i * quarter : (i + 1) * quarter, 0:n] for i in range(4)]

    def make_kv(p):
        raw = lax.dot_general(tok[p], wkv[...], (((1,), (1,)), ((), ())), preferred_element_type=F32)
        turned = jnp.transpose(raw)
        gain = gain_cols[:, heads * rows : heads * rows + rows]
        keys = prepare(turned[0:width], gain, tables_of(p, rows))
        to = kv_rows(p, 0, core, 0)
        kv[to, 0:width] = jnp.transpose(keys).astype(BF16)
        kv[to, width : 2 * width] = raw[:, width:].astype(BF16)

    def make_queries(p):
        raw = jnp.dot(tok[p], wq[...], preferred_element_type=F32)
        stacked = jnp.concatenate([raw[:, h * width : (h + 1) * width] for h in range(heads)], axis=0)
        q = prepare(jnp.transpose(stacked), gain_cols[:, 0 : heads * rows], tables_of(p, heads * rows))
        at = slice((p % 2) * heads * rows, (p % 2 + 1) * heads * rows)
        queries[p // 2, :, at] = q.astype(BF16)

    def kv_copy(p, j, k, to_j, to_k, slot, where):
        return send(
            kv.at[kv_rows(p, j, core, k)],
            kv.at[kv_rows(p, to_j, core, to_k)],
            kv_send.at[p, slot],
            kv_recv.at[p, to_j, core, to_k],
            where,
        )

    def own_copies(p):
        copies = [kv_copy(p, 0, 0, 0, RING - i, i - 1, peer_a(i)) for i in range(1, RING)]
        copies += [kv_copy(p, 0, 0, RING - i, 0, i + 2, peer_b(i)) for i in range(1, RING)]
        return copies + [kv_copy(p, 0, 0, 0, 0, 6, to_mate)]

    def spread_copies(p, k):
        base = 7 + (k - 1) * RING
        copies = [kv_copy(p, 0, k, RING - i, k, base + i - 1, peer_b(i)) for i in range(1, RING)]
        return copies + [kv_copy(p, 0, k, 0, k, base + RING - 1, to_mate)]

    def hand_copies(p, j):
        return [kv_copy(p, j, k, j, k, 19 + (j - 1) * RING + k, to_mate) for k in range(RING)]

    def own_send(p):
        for copy in own_copies(p):
            copy.start()

    def spread(p):
        for k in (1, 3, 2):
            copies = spread_copies(p, k)
            copies[-1].wait_recv()
            for copy in copies:
                copy.start()

    def hand(p, j):
        for copy in hand_copies(p, j):
            copy.wait_recv()
            copy.start()

    def from_mate(p, j):
        for k in range(RING):
            spot = kv.at[kv_rows(p, j, 1 - core, k)]
            send(spot, spot, kv_send.at[p, 0], kv_recv.at[p, j, 1 - core, k], to_mate).wait_recv()

    piece_rows = group // 4

    def wo_copy(block, to_block, side, i, slot, where):
        at = pl.ds(pl.multiple_of((side * 2 + i) * piece_rows, piece_rows), piece_rows)
        return send(
            wo.at[block, at], wo.at[to_block, at], wo_send.at[slot], wo_recv.at[to_block, side, i], where
        )

    wo_out = [
        wo_copy(0, 1, core, 0, 0, to_right),
        wo_copy(0, 2, core, 1, 1, to_left),
        wo_copy(0, 1, core, 1, 2, to_right),
        wo_copy(0, 2, core, 0, 3, to_left),
    ]
    wo_on = [wo_copy(1, 3, core, 0, 4, to_right), wo_copy(2, 3, core, 1, 5, to_left)]
    wo_order = ((1, 0), (2, 1), (1, 1), (2, 0), (3, 0), (3, 1))
    wo_hand = [wo_copy(block, block, core, i, 6 + n, to_mate) for n, (block, i) in enumerate(wo_order)]

    def piece_work(p):
        make_kv(p)
        own_send(p)
        make_queries(p)

    loads[0].wait()
    loads[1].wait()
    loads[2].wait()
    make_kv(0)
    own_send(0)
    loads[3].wait()
    make_queries(0)
    spread(0)
    for i, copy in enumerate(token_on):
        token_wait(1, i)
        copy.start()
    piece_work(1)
    from_mate(0, 0)

    def turn(chunk, slot):
        at = pl.ds(pl.multiple_of(chunk * CHUNK, CHUNK), CHUNK)
        turned_v[slot, 0:width] = jnp.transpose(kv[at])[width : 2 * width]

    def score(chunk, side, t, slot, i):
        at = pl.ds(pl.multiple_of(chunk * CHUNK + i * SUB, SUB), SUB)
        q = queries[side, :, t * TILE : (t + 1) * TILE]
        s = jnp.dot(kv[at, 0:width], q, preferred_element_type=F32)
        scores[slot, i * SUB : (i + 1) * SUB] = s
        return jnp.max(s.reshape(SUB // 8, 8, TILE), axis=0)

    def score_all(chunk, side, t, slot):
        best = None
        for i in range(CHUNK // SUB):
            m = score(chunk, side, t, slot, i)
            best = m if best is None else jnp.maximum(best, m)
        peak[slot] = best

    n_steps = 2 * 4 * RING

    def chunk_of(s):
        late = s // 16
        return (1 - late) * lax.rem(s, 8) + late * (8 + 4 * (lax.rem(s, 16) // 8) + lax.rem(s, 4))

    def side_of(s):
        late = s // 16
        return (1 - late) * (s // 8) + late * (1 - lax.rem(s // 4, 2))

    turn(0, 0)
    score_all(0, 0, 0, 0)
    score_all(0, 0, 1, 1)

    def finish(side):
        flat = [acc[side, t] for t in range(n_tiles)]
        sums = jnp.concatenate([f[width : width + 8] for f in flat], axis=1)
        tops = jnp.concatenate([top[side, t] for t in range(n_tiles)], axis=1)
        outs = jnp.concatenate([f[0:width] / f[width : width + 1] for f in flat], axis=1)
        logs = (tops + jnp.log2(sums)) * LN2
        turned = jnp.transpose(jnp.concatenate([outs, logs], axis=0))
        for q in range(2):
            p = 2 * side + q
            for h in range(heads):
                base = (q * heads + h) * rows
                att[p, :, h * width : (h + 1) * width] = turned[base : base + rows, 0:width].astype(BF16)
        return turned

    def keep_logs(side, turned):
        for q in range(2):
            for h in range(heads):
                for i in range(2):
                    base = (q * heads + h) * rows + i * half
                    to = pl.ds(pl.multiple_of(starts[2 * side + q][i], half), half)
                    log_rows[to, h : h + 1] = turned[base : base + half, width : width + 1]

    def att_copy(p, i, source, at, slot, where):
        src = att.at[p] if i is None else att.at[p, part(i)]
        dst = att_in.at[source] if at is None else att_in.at[source, part(at)]
        return send(src, dst, att_send.at[slot], att_recv.at[source, at or 0], where)

    att_late = [
        att_copy(3, None, 2, None, 0, to_opposite),
        att_copy(2, 0, 1, 1, 1, to_left),
        att_copy(2, 1, 0, 0, 2, to_right),
    ]
    att_last = [att_copy(1, 0, 1, 0, 3, to_left), att_copy(1, 1, 0, 1, 4, to_right)]

    def at_step(s, now, acts):
        @pl.when(s == now)
        def _():
            for act in acts:
                act()

    def wait_tokens(p):
        for i in range(2):
            token_wait(p, i)

    def start_wo():
        loads[4].wait()
        for copy in wo_out:
            copy.start()

    def wo_first():
        for n in range(2):
            wo_hand[n].wait_recv()
            wo_on[n].start()
            wo_hand[n].start()

    def close_late():
        keep_logs(1, finish(1))
        for copy in att_late:
            copy.start()

    def later(f, *args):
        return functools.partial(f, *args)

    duties = {
        0: [later(hand, 0, j) for j in (1, 2, 3)] + [later(from_mate, 0, 1)],
        1: [later(wait_tokens, 2), later(piece_work, 2), later(spread, 1), later(from_mate, 0, 2)],
        2: [later(from_mate, 0, 3)],
        3: [later(from_mate, 1, 0)],
        4: [later(hand, 1, j) for j in (1, 2, 3)] + [later(from_mate, 1, 1)],
        5: [later(from_mate, 1, 2), later(spread, 2)],
        6: [later(from_mate, 1, 3)],
        7: [later(wait_tokens, 3), later(piece_work, 3), start_wo],
        12: [later(hand, 2, j) for j in (1, 2, 3)],
        13: [later(spread, 3)],
        15: [later(from_mate, 2, 0)],
        16: [later(from_mate, 2, 1)],
        17: [later(from_mate, 2, 2)],
        18: [later(from_mate, 2, 3)],
        21: [later(hand, 3, j) for j in (1, 2, 3)],
        22: [wo_first],
        23: [later(from_mate, 3, 0)],
        24: [later(from_mate, 3, 1)],
        25: [later(from_mate, 3, 2)],
        26: [later(from_mate, 3, 3)],
        28: [close_late],
    }

    def step(s, carry):
        for now, acts in duties.items():
            if acts:
                at_step(s, now, acts)
        slot_v = lax.rem(s, 2)
        after = lax.rem(s + 1, n_steps)
        chunk, side = chunk_of(s), side_of(s)
        next_chunk, next_side = chunk_of(after), side_of(after)
        for t in range(n_tiles):
            if t == 1:
                turn(next_chunk, 1 - slot_v)
            ahead = t + 2
            to_chunk, to_side = (chunk, side) if ahead < n_tiles else (next_chunk, next_side)
            tile, fill, slot = ahead % n_tiles, ahead % 3, t % 3
            old = top[side, t]
            new = jnp.maximum(old, jnp.max(peak[slot], axis=0, keepdims=True))
            best = None
            total = None
            for i in range(CHUNK // SUB):
                m = score(to_chunk, to_side, tile, fill, i)
                best = m if best is None else jnp.maximum(best, m)
                at = slice(i * SUB, (i + 1) * SUB)
                weights = jnp.exp2(scores[slot, at] - new).astype(BF16)
                mixed = jnp.dot(turned_v[slot_v, :, at], weights, preferred_element_type=F32)
                total = mixed if total is None else total + mixed
            peak[fill] = best
            acc[side, t] = acc[side, t] * jnp.exp2(old - new) + total
            top[side, t] = new
        return carry

    lax.fori_loop(0, n_steps, step, 0)

    turned = finish(0)
    for copy in att_last:
        copy.start()
    keep_logs(0, turned)
    log_ref[...] = jnp.transpose(log_rows[...])[0:heads]

    for n in range(2, 6):
        wo_hand[n].wait_recv()
        wo_hand[n].start()
    for block, i in wo_order:
        wo_copy(block, block, 1 - core, i, 0, to_mate).wait_recv()

    cols = 512

    def columns(n):
        return slice(n * cols, (n + 1) * cols)

    def times(x, block, n):
        return jnp.dot(x, wo[block, :, columns(n)], preferred_element_type=F32)

    att_late[0].wait_recv()
    for n in range(model // cols):
        product[:, columns(n)] = times(att[0], 0, n) + times(att_in[2], 3, n)
    for copy in att_late[1:] + att_last:
        copy.wait_recv()
    for n in range(model // cols):
        total = product[:, columns(n)] + times(att_in[0], 1, n) + times(att_in[1], 2, n)
        mixed_ref[:, columns(n)] = total.astype(BF16)

    for copy in token_out + token_on + wo_out + wo_on + wo_hand + att_late + att_last:
        copy.wait_send()
    for p in range(4):
        copies = own_copies(p)
        for k in range(1, RING):
            copies += spread_copies(p, k) + hand_copies(p, k)
        for copy in copies:
            copy.wait_send()


def body(tokens, query_weight, key_weight, value_weight, out_weight, query_gain, key_gain):
    rows, depth = tokens.shape
    query_cols = query_weight.shape[1]
    kv_cols = key_weight.shape[1]
    heads, width = query_gain.shape
    group, model = out_weight.shape
    count = rows * RING
    n_sp = RING * RING * 2
    n_tiles = 2 * heads * rows // TILE
    any_space = pl.BlockSpec(memory_space=pl.ANY)
    vmem = pl.BlockSpec(memory_space=pltpu.VMEM)
    dma = pltpu.SemaphoreType.DMA
    return pl.pallas_call(
        kernel,
        out_shape=(
            pltpu.VMEM((rows, model), BF16),
            pltpu.VMEM((heads, count), F32),
        ),
        in_specs=[any_space] * 5 + [vmem] * 2,
        out_specs=(vmem, vmem),
        scratch_shapes=[
            pltpu.VMEM((4, rows, depth), BF16),
            pltpu.VMEM((depth, query_cols), BF16),
            pltpu.VMEM((2 * kv_cols, depth), BF16),
            pltpu.VMEM((4, group, model), BF16),
            pltpu.VMEM((width, heads * rows + 128), F32),
            pltpu.VMEM((4, width, heads * rows), F32),
            pltpu.VMEM((2, width, 2 * heads * rows), BF16),
            pltpu.VMEM((n_sp * count, 2 * width), BF16),
            pltpu.VMEM((3, CHUNK, TILE), F32),
            pltpu.VMEM((3, 8, TILE), F32),
            pltpu.VMEM((2, width + ONES, CHUNK), BF16),
            pltpu.VMEM((2, n_tiles, width + ONES, TILE), F32),
            pltpu.VMEM((2, n_tiles, 1, TILE), F32),
            pltpu.VMEM((4, rows, group), BF16),
            pltpu.VMEM((3, rows, group), BF16),
            pltpu.VMEM((count, 128), F32),
            pltpu.VMEM((rows, model), F32),
            dma((5,)),
            dma((6,)),
            dma((4, 2)),
            dma((4, 31)),
            dma((4, RING, 2, RING)),
            dma((12,)),
            dma((4, 2, 2)),
            dma((5,)),
            dma((3, 2)),
        ],
        compiler_params=pltpu.CompilerParams(
            collective_id=0, has_side_effects=True, vmem_limit_bytes=60 * 1024 * 1024
        ),
        name="attention",
    )(tokens, query_weight, key_weight.T, value_weight.T, out_weight, query_gain, key_gain)


def solution(mesh):
    return jax.shard_map(
        body,
        mesh=mesh,
        in_specs=(
            P(("sp", "tp"), None),
            P(None, "tp"),
            P(None, "tp"),
            P(None, "tp"),
            P("tp", None),
            P("tp", None),
            P("tp", None),
        ),
        out_specs=(P(("sp", "tp"), None), P("tp", "sp")),
        check_vma=False,
    )
```

time: 59.3 us -> 59.4 us (level)
  no operation moved by 1% of the time
where the time goes in v2:
time: 59.4 us; the launch traced here: 59.3 us
  Pallas kernels  57.3 us (96%)
  local copies, waits for them, and re-layouts  1.34 us (2%)
  between operations  0.64 us (1%)
    pallas_call x1, Pallas kernels, body(): pl.pallas_call(kernel, out_shape=(pltpu.VMEM((rows, model), BF16), pltpu....  57.3 us
    unnamed x2, local copies, waits for them, and re-layouts  1.34 us

profile of v2, /device:TPU:1, one launch (start us, length us, event | category | flops | bytes accessed | tf_op | source)
XLA Modules:
  0.0 59.3 jit_solution(12395666430270699819)
XLA Ops:
  0.6 57.3 %attention.1 = (bf16[96,2048]{1,0:T(8,128)(2,1)S(1)}, f32[4,384]{1,0:T(4,128)S(1)}) custom-call(bf16[96,2048]{1,0:T(8,128)(2,1)} %tok_hbm.1, bf16[2048,256]{1,0:T(8,128)(2,1)} %wq_hbm.1, bf16[64,2048]{1,0:T(8,128)(2,1)} %bitcast.2, bf16[64,2048]{1,0:T(8,128)(2,1)} %bitcast.3, bf16[256,2048]{1,0:T(8,128)(2,1)} %wo_hbm.1, bf16[4,64]{1,0:T(4,128)(2,1)} %qg_ref.1, ...), custom_call_target="tpu_custom_call" | custom-call | tf_op jit(solution)/shard_map/attention/pallas_call | solution.py:503
  57.9 0.7 %copy.11 = bf16[96,2048]{1,0:T(8,128)(2,1)} copy(bf16[96,2048]{1,0:T(8,128)(2,1)S(1)} %get-tuple-element.2) | data formatting | bytes 786432
  58.7 0.6 %copy.12 = f32[4,384]{1,0:T(4,128)} copy(f32[4,384]{1,0:T(4,128)S(1)} %get-tuple-element.3) | data formatting | bytes 12288

commit v3 on v2

--- a/solution.py
+++ b/solution.py
@@ -196,8 +196,11 @@
     turned_v[:, width:, :] = jnp.ones_like(turned_v[:, width:, :])
     log_rows[...] = jnp.zeros_like(log_rows)
 
-    def kv_rows(p, j, c, k):
-        return pl.ds(pl.multiple_of((((p * RING + j) * 2 + c) * RING + k) * rows, rows), rows)
+    place_of = (0, 1, 3, 2)
+
+    def kv_rows(p, shift, c, k, n):
+        base = (((p * RING + place_of[shift]) * 2 + c) * RING + k) * rows
+        return kv.at[pl.ds(pl.multiple_of(base, half), n)]
 
     def tables_of(p, n):
         return [tables[p, i * quarter : (i + 1) * quarter, 0:n] for i in range(4)]
@@ -207,9 +210,9 @@
         turned = jnp.transpose(raw)
         gain = gain_cols[:, heads * rows : heads * rows + rows]
         keys = prepare(turned[0:width], gain, tables_of(p, rows))
-        to = kv_rows(p, 0, core, 0)
-        kv[to, 0:width] = jnp.transpose(keys).astype(BF16)
-        kv[to, width : 2 * width] = raw[:, width:].astype(BF16)
+        to = kv_rows(p, 0, core, 0, rows)
+        to[:, 0:width] = jnp.transpose(keys).astype(BF16)
+        to[:, width : 2 * width] = raw[:, width:].astype(BF16)
 
     def make_queries(p):
         raw = jnp.dot(tok[p], wq[...], preferred_element_type=F32)
@@ -218,66 +221,72 @@
         at = slice((p % 2) * heads * rows, (p % 2 + 1) * heads * rows)
         queries[p // 2, :, at] = q.astype(BF16)
 
-    def kv_copy(p, j, k, to_j, to_k, slot, where):
+    def kv_copy(src, dst, p, shift, c, where):
+        return send(src, dst, kv_send.at[p], kv_recv.at[p, place_of[shift], c], where)
+
+    whole = RING * rows
+
+    def own_send(p):
+        src = kv_rows(p, 0, core, 0, rows)
+        for i in (1, 3, 2):
+            kv_copy(src, kv_rows(p, 0, core, RING - i, rows), p, 0, core, peer_a(i)).start()
+
+    def hand_copy(p, shift):
+        spot = kv_rows(p, shift, core, 0, whole)
+        return kv_copy(spot, spot, p, shift, core, to_mate)
+
+    def spread(p):
+        spot = kv_rows(p, 0, core, 1, whole - rows)
+        kv_copy(spot, spot, p, 0, core, to_mate).wait_recv()
+        src = kv_rows(p, 0, core, 0, whole)
+        for i in (1, 3):
+            kv_copy(src, kv_rows(p, RING - i, core, 0, whole), p, RING - i, core, peer_b(i)).start()
+        hand_copy(p, 0).start()
+
+    def relay(p):
+        for shift, k, to in ((3, 0, 1), (1, 2, 3)):
+            hand_copy(p, shift).wait_recv()
+            src = kv_rows(p, shift, core, k, 2 * rows)
+            kv_copy(src, kv_rows(p, 2, core, k, 2 * rows), p, 2, core, peer_b(to)).start()
+            hand_copy(p, shift).start()
+
+    def hand(p):
+        hand_copy(p, 2).wait_recv()
+        hand_copy(p, 2).start()
+
+    def from_mate(p, shift):
+        spot = kv_rows(p, shift, 1 - core, 0, whole)
+        kv_copy(spot, spot, p, shift, 1 - core, to_mate).wait_recv()
+
+    strip = group // 8
+    parity = lax.rem(coord_a, 2)
+    to_pair = {"sp": sp + (1 - 2 * parity) * step_a}
+
+    def wo_rows(block, side, first, n):
+        return wo.at[block, pl.ds(pl.multiple_of((side * 4 + first) * strip, strip), n * strip)]
+
+    def wo_copy(block, to_block, i, slot, where):
+        at = 2 * parity + i
         return send(
-            kv.at[kv_rows(p, j, core, k)],
-            kv.at[kv_rows(p, to_j, core, to_k)],
-            kv_send.at[p, slot],
-            kv_recv.at[p, to_j, core, to_k],
-            where,
+            wo_rows(block, core, at, 1), wo_rows(to_block, core, at, 1), wo_send.at[slot], wo_recv.at[to_block, i], where
         )
 
-    def own_copies(p):
-        copies = [kv_copy(p, 0, 0, 0, RING - i, i - 1, peer_a(i)) for i in range(1, RING)]
-        copies += [kv_copy(p, 0, 0, RING - i, 0, i + 2, peer_b(i)) for i in range(1, RING)]
-        return copies + [kv_copy(p, 0, 0, 0, 0, 6, to_mate)]
-
-    def spread_copies(p, k):
-        base = 7 + (k - 1) * RING
-        copies = [kv_copy(p, 0, k, RING - i, k, base + i - 1, peer_b(i)) for i in range(1, RING)]
-        return copies + [kv_copy(p, 0, k, 0, k, base + RING - 1, to_mate)]
-
-    def hand_copies(p, j):
-        return [kv_copy(p, j, k, j, k, 19 + (j - 1) * RING + k, to_mate) for k in range(RING)]
-
-    def own_send(p):
-        for copy in own_copies(p):
-            copy.start()
-
-    def spread(p):
-        for k in (1, 3, 2):
-            copies = spread_copies(p, k)
-            copies[-1].wait_recv()
-            for copy in copies:
-                copy.start()
-
-    def hand(p, j):
-        for copy in hand_copies(p, j):
-            copy.wait_recv()
-            copy.start()
-
-    def from_mate(p, j):
-        for k in range(RING):
-            spot = kv.at[kv_rows(p, j, 1 - core, k)]
-            send(spot, spot, kv_send.at[p, 0], kv_recv.at[p, j, 1 - core, k], to_mate).wait_recv()
-
-    piece_rows = group // 4
-
-    def wo_copy(block, to_block, side, i, slot, where):
-        at = pl.ds(pl.multiple_of((side * 2 + i) * piece_rows, piece_rows), piece_rows)
-        return send(
-            wo.at[block, at], wo.at[to_block, at], wo_send.at[slot], wo_recv.at[to_block, side, i], where
-        )
-
     wo_out = [
-        wo_copy(0, 1, core, 0, 0, to_right),
-        wo_copy(0, 2, core, 1, 1, to_left),
-        wo_copy(0, 1, core, 1, 2, to_right),
-        wo_copy(0, 2, core, 0, 3, to_left),
+        wo_copy(0, 1, 0, 0, to_right),
+        wo_copy(0, 2, 1, 1, to_left),
+        wo_copy(0, 1, 1, 2, to_right),
+        wo_copy(0, 2, 0, 3, to_left),
     ]
-    wo_on = [wo_copy(1, 3, core, 0, 4, to_right), wo_copy(2, 3, core, 1, 5, to_left)]
-    wo_order = ((1, 0), (2, 1), (1, 1), (2, 0), (3, 0), (3, 1))
-    wo_hand = [wo_copy(block, block, core, i, 6 + n, to_mate) for n, (block, i) in enumerate(wo_order)]
+    wo_on = [wo_copy(1, 3, 0, 4, to_right), wo_copy(2, 3, 1, 5, to_left)]
+    wo_rest = [wo_copy(0, 1, 1, 2, to_right), wo_copy(0, 2, 0, 3, to_left)]
+
+    def pair_copy(block):
+        spot = wo_rows(block, core, 2 * parity, 2)
+        return send(spot, spot, wo_send.at[5 + block], wo_recv.at[block, 2], to_pair)
+
+    def wo_hand(block):
+        spot = wo_rows(block, core, 0, 4)
+        return send(spot, spot, wo_send.at[8 + block], wo_recv.at[block, 3], to_mate)
 
     def piece_work(p):
         make_kv(p)
@@ -295,7 +304,11 @@
     for i, copy in enumerate(token_on):
         token_wait(1, i)
         copy.start()
+    loads[4].wait()
+    for copy in wo_out:
+        copy.start()
     piece_work(1)
+    relay(0)
     from_mate(0, 0)
 
     def turn(chunk, slot):
@@ -319,12 +332,12 @@
     n_steps = 2 * 4 * RING
 
     def chunk_of(s):
-        late = s // 16
-        return (1 - late) * lax.rem(s, 8) + late * (8 + 4 * (lax.rem(s, 16) // 8) + lax.rem(s, 4))
+        mid, end = (s + 22) // 32, (s + 8) // 32
+        return (1 - mid) * lax.rem(s, 5) + (mid - end) * (s // 2) + end * (12 + lax.rem(s, 4))
 
     def side_of(s):
-        late = s // 16
-        return (1 - late) * (s // 8) + late * (1 - lax.rem(s // 4, 2))
+        mid, end = (s + 22) // 32, (s + 8) // 32
+        return (1 - mid) * (s // 5) + (mid - end) * lax.rem(s, 2) + end * (1 - lax.rem(s // 4, 2))
 
     turn(0, 0)
     score_all(0, 0, 0, 0)
@@ -374,16 +387,26 @@
         for i in range(2):
             token_wait(p, i)
 
-    def start_wo():
-        loads[4].wait()
-        for copy in wo_out:
-            copy.start()
-
-    def wo_first():
-        for n in range(2):
-            wo_hand[n].wait_recv()
-            wo_on[n].start()
-            wo_hand[n].start()
+    def wo_one():
+        wo_copy(1, 1, 0, 4, to_right).wait_recv()
+        wo_on[0].start()
+        wo_copy(2, 2, 1, 5, to_left).wait_recv()
+        wo_on[1].start()
+
+    def wo_two():
+        for copy, block in zip(wo_rest, (1, 2)):
+            copy.wait_recv()
+            pair_copy(block).start()
+
+    def wo_three():
+        for copy in wo_on:
+            copy.wait_recv()
+        pair_copy(3).start()
+
+    def wo_swap(*blocks):
+        for block in blocks:
+            pair_copy(block).wait_recv()
+            wo_hand(block).start()
 
     def close_late():
         keep_logs(1, finish(1))
@@ -394,27 +417,32 @@
         return functools.partial(f, *args)
 
     duties = {
-        0: [later(hand, 0, j) for j in (1, 2, 3)] + [later(from_mate, 0, 1)],
-        1: [later(wait_tokens, 2), later(piece_work, 2), later(spread, 1), later(from_mate, 0, 2)],
-        2: [later(from_mate, 0, 3)],
+        0: [later(from_mate, 0, 1)],
+        1: [later(from_mate, 0, 3), later(wait_tokens, 2), later(piece_work, 2)],
+        2: [later(hand, 0), later(spread, 1), later(from_mate, 0, 2)],
         3: [later(from_mate, 1, 0)],
-        4: [later(hand, 1, j) for j in (1, 2, 3)] + [later(from_mate, 1, 1)],
-        5: [later(from_mate, 1, 2), later(spread, 2)],
-        6: [later(from_mate, 1, 3)],
-        7: [later(wait_tokens, 3), later(piece_work, 3), start_wo],
-        12: [later(hand, 2, j) for j in (1, 2, 3)],
-        13: [later(spread, 3)],
+        4: [later(wait_tokens, 3), later(piece_work, 3), later(relay, 1)],
+        5: [later(spread, 2)],
+        8: [later(hand, 1)],
+        9: [later(from_mate, 1, 1)],
+        10: [later(relay, 2)],
+        11: [later(from_mate, 1, 3)],
+        12: [later(spread, 3)],
+        13: [later(from_mate, 1, 2), wo_one],
         15: [later(from_mate, 2, 0)],
-        16: [later(from_mate, 2, 1)],
-        17: [later(from_mate, 2, 2)],
-        18: [later(from_mate, 2, 3)],
-        21: [later(hand, 3, j) for j in (1, 2, 3)],
-        22: [wo_first],
+        16: [later(hand, 2)],
+        17: [later(from_mate, 2, 1)],
+        18: [wo_two],
+        19: [later(from_mate, 2, 3)],
+        20: [later(relay, 3)],
+        21: [later(from_mate, 2, 2)],
+        22: [wo_three],
         23: [later(from_mate, 3, 0)],
         24: [later(from_mate, 3, 1)],
-        25: [later(from_mate, 3, 2)],
-        26: [later(from_mate, 3, 3)],
+        25: [later(from_mate, 3, 3)],
+        26: [later(hand, 3), later(wo_swap, 1, 2), later(from_mate, 3, 2)],
         28: [close_late],
+        29: [later(wo_swap, 3)],
     }
 
     def step(s, carry):
@@ -455,11 +483,9 @@
     keep_logs(0, turned)
     log_ref[...] = jnp.transpose(log_rows[...])[0:heads]
 
-    for n in range(2, 6):
-        wo_hand[n].wait_recv()
-        wo_hand[n].start()
-    for block, i in wo_order:
-        wo_copy(block, block, 1 - core, i, 0, to_mate).wait_recv()
+    for block in (1, 2, 3):
+        other = wo_rows(block, 1 - core, 0, 4)
+        send(other, other, wo_send.at[0], wo_recv.at[block, 3], to_mate).wait_recv()
 
     cols = 512
 
@@ -478,14 +504,14 @@
         total = product[:, columns(n)] + times(att_in[0], 1, n) + times(att_in[1], 2, n)
         mixed_ref[:, columns(n)] = total.astype(BF16)
 
-    for copy in token_out + token_on + wo_out + wo_on + wo_hand + att_late + att_last:
+    for copy in token_out + token_on + wo_out + wo_on + att_late + att_last:
         copy.wait_send()
+    for block in (1, 2, 3):
+        pair_copy(block).wait_send()
+        wo_hand(block).wait_send()
     for p in range(4):
-        copies = own_copies(p)
-        for k in range(1, RING):
-            copies += spread_copies(p, k) + hand_copies(p, k)
-        for copy in copies:
-            copy.wait_send()
+        sent = kv.at[pl.ds(0, 31 * rows)]
+        kv_copy(sent, sent, p, 0, core, to_mate).wait_send()
 
 
 def body(tokens, query_weight, key_weight, value_weight, out_weight, query_gain, key_gain):
@@ -529,10 +555,10 @@
             dma((5,)),
             dma((6,)),
             dma((4, 2)),
-            dma((4, 31)),
-            dma((4, RING, 2, RING)),
+            dma((4,)),
+            dma((4, RING, 2)),
             dma((12,)),
-            dma((4, 2, 2)),
+            dma((4, 4)),
             dma((5,)),
             dma((3, 2)),
         ],

time: 59.4 us -> 60.8 us (1.024)
  Pallas kernels: 57.3 us -> 58.7 us
    pallas_call x1, Pallas kernels: 57.3 us -> 58.7 us  [body(): pl.pallas_call(kernel, out_shape=(pltpu.VMEM((rows, model), BF16), pltpu....]
where the time goes in v3:
time: 60.8 us; the launch traced here: 60.6 us
  Pallas kernels  58.7 us (97%)
  local copies, waits for them, and re-layouts  1.34 us (2%)
  between operations  0.64 us (1%)
    pallas_call x1, Pallas kernels, body(): pl.pallas_call(kernel, out_shape=(pltpu.VMEM((rows, model), BF16), pltpu....  58.7 us
    unnamed x2, local copies, waits for them, and re-layouts  1.34 us

profile of v3, /device:TPU:1, one launch (start us, length us, event | category | flops | bytes accessed | tf_op | source)
XLA Modules:
  0.0 60.6 jit_solution(18389287205558274728)
XLA Ops:
  0.6 58.7 %attention.1 = (bf16[96,2048]{1,0:T(8,128)(2,1)S(1)}, f32[4,384]{1,0:T(4,128)S(1)}) custom-call(bf16[96,2048]{1,0:T(8,128)(2,1)} %tok_hbm.1, bf16[2048,256]{1,0:T(8,128)(2,1)} %wq_hbm.1, bf16[64,2048]{1,0:T(8,128)(2,1)} %bitcast.2, bf16[64,2048]{1,0:T(8,128)(2,1)} %bitcast.3, bf16[256,2048]{1,0:T(8,128)(2,1)} %wo_hbm.1, bf16[4,64]{1,0:T(4,128)(2,1)} %qg_ref.1, ...), custom_call_target="tpu_custom_call" | custom-call | tf_op jit(solution)/shard_map/attention/pallas_call | solution.py:529
  59.3 0.7 %copy.11 = bf16[96,2048]{1,0:T(8,128)(2,1)} copy(bf16[96,2048]{1,0:T(8,128)(2,1)S(1)} %get-tuple-element.2) | data formatting | bytes 786432
  60.0 0.6 copy.12

commit v4 on v3

--- a/solution.py
+++ b/solution.py
@@ -79,6 +79,9 @@
     sp = lax.axis_index("sp")
     tp = lax.axis_index("tp")
     core = lax.rem(sp, 2)
+    scores, peak, turned_v, acc, top, queries = (
+        ref.at[core] for ref in (scores, peak, turned_v, acc, top, queries)
+    )
     y = lax.rem(sp // 2, RING)
     z = sp // (2 * RING)
     mate = sp + 1 - 2 * core
@@ -329,20 +332,6 @@
             best = m if best is None else jnp.maximum(best, m)
         peak[slot] = best
 
-    n_steps = 2 * 4 * RING
-
-    def chunk_of(s):
-        mid, end = (s + 22) // 32, (s + 8) // 32
-        return (1 - mid) * lax.rem(s, 5) + (mid - end) * (s // 2) + end * (12 + lax.rem(s, 4))
-
-    def side_of(s):
-        mid, end = (s + 22) // 32, (s + 8) // 32
-        return (1 - mid) * (s // 5) + (mid - end) * lax.rem(s, 2) + end * (1 - lax.rem(s // 4, 2))
-
-    turn(0, 0)
-    score_all(0, 0, 0, 0)
-    score_all(0, 0, 1, 1)
-
     def finish(side):
         flat = [acc[side, t] for t in range(n_tiles)]
         sums = jnp.concatenate([f[width : width + 8] for f in flat], axis=1)
@@ -377,12 +366,6 @@
     ]
     att_last = [att_copy(1, 0, 1, 0, 3, to_left), att_copy(1, 1, 0, 1, 4, to_right)]
 
-    def at_step(s, now, acts):
-        @pl.when(s == now)
-        def _():
-            for act in acts:
-                act()
-
     def wait_tokens(p):
         for i in range(2):
             token_wait(p, i)
@@ -413,69 +396,113 @@
         for copy in att_late:
             copy.start()
 
-    def later(f, *args):
-        return functools.partial(f, *args)
-
-    duties = {
-        0: [later(from_mate, 0, 1)],
-        1: [later(from_mate, 0, 3), later(wait_tokens, 2), later(piece_work, 2)],
-        2: [later(hand, 0), later(spread, 1), later(from_mate, 0, 2)],
-        3: [later(from_mate, 1, 0)],
-        4: [later(wait_tokens, 3), later(piece_work, 3), later(relay, 1)],
-        5: [later(spread, 2)],
-        8: [later(hand, 1)],
-        9: [later(from_mate, 1, 1)],
-        10: [later(relay, 2)],
-        11: [later(from_mate, 1, 3)],
-        12: [later(spread, 3)],
-        13: [later(from_mate, 1, 2), wo_one],
-        15: [later(from_mate, 2, 0)],
-        16: [later(hand, 2)],
-        17: [later(from_mate, 2, 1)],
-        18: [wo_two],
-        19: [later(from_mate, 2, 3)],
-        20: [later(relay, 3)],
-        21: [later(from_mate, 2, 2)],
-        22: [wo_three],
-        23: [later(from_mate, 3, 0)],
-        24: [later(from_mate, 3, 1)],
-        25: [later(from_mate, 3, 3)],
-        26: [later(hand, 3), later(wo_swap, 1, 2), later(from_mate, 3, 2)],
-        28: [close_late],
-        29: [later(wo_swap, 3)],
-    }
-
-    def step(s, carry):
-        for now, acts in duties.items():
-            if acts:
-                at_step(s, now, acts)
-        slot_v = lax.rem(s, 2)
-        after = lax.rem(s + 1, n_steps)
-        chunk, side = chunk_of(s), side_of(s)
-        next_chunk, next_side = chunk_of(after), side_of(after)
+    def items(side, *spots):
+        return [(p * RING + place_of[shift], side) for p, shift in spots]
+
+    def both(*spots):
+        return [item for spot in spots for item in items(1, spot) + items(0, spot)]
+
+    def attend(item, after, slot_v):
+        chunk, side = item
         for t in range(n_tiles):
-            if t == 1:
-                turn(next_chunk, 1 - slot_v)
             ahead = t + 2
-            to_chunk, to_side = (chunk, side) if ahead < n_tiles else (next_chunk, next_side)
+            target = item if ahead < n_tiles else after
+            if t == 1 and after is not None:
+                turn(after[0], 1 - slot_v)
             tile, fill, slot = ahead % n_tiles, ahead % 3, t % 3
             old = top[side, t]
             new = jnp.maximum(old, jnp.max(peak[slot], axis=0, keepdims=True))
             best = None
             total = None
             for i in range(CHUNK // SUB):
-                m = score(to_chunk, to_side, tile, fill, i)
-                best = m if best is None else jnp.maximum(best, m)
+                if target is not None:
+                    m = score(target[0], target[1], tile, fill, i)
+                    best = m if best is None else jnp.maximum(best, m)
                 at = slice(i * SUB, (i + 1) * SUB)
                 weights = jnp.exp2(scores[slot, at] - new).astype(BF16)
                 mixed = jnp.dot(turned_v[slot_v, :, at], weights, preferred_element_type=F32)
                 total = mixed if total is None else total + mixed
-            peak[fill] = best
+            if target is not None:
+                peak[fill] = best
             acc[side, t] = acc[side, t] * jnp.exp2(old - new) + total
             top[side, t] = new
-        return carry
-
-    lax.fori_loop(0, n_steps, step, 0)
+
+    def run(todo, slot_v, after=None, cold=False):
+        if cold:
+            turn(todo[0][0], slot_v)
+            for t in range(2):
+                score_all(todo[0][0], todo[0][1], t, t)
+        for n, item in enumerate(todo):
+            attend(item, todo[n + 1] if n + 1 < len(todo) else after, (slot_v + n) % 2)
+        return (slot_v + len(todo)) % 2
+
+    def next_piece(p):
+        wait_tokens(p)
+        piece_work(p)
+
+    def mates(*spots):
+        for spot in spots:
+            from_mate(*spot)
+
+    next_piece(2)
+    spread(1)
+    mates((0, 1), (0, 3))
+    run(items(0, (0, 0), (0, 1), (0, 3)), 0, cold=True)
+    hand(0)
+    from_mate(1, 0)
+    run(items(0, (1, 0)), 0, cold=True)
+    next_piece(3)
+    relay(1)
+    spread(2)
+    from_mate(0, 2)
+    plan = [
+        items(1, (0, 0), (0, 1), (0, 3)),
+        both((0, 2)) + items(1, (1, 0)),
+        both((1, 1), (1, 3)),
+        both((2, 0)) + items(1, (1, 2)),
+        items(0, (1, 2)) + both((2, 1)) + items(1, (2, 3)),
+        items(0, (2, 3)) + items(1, (3, 0)),
+        items(0, (3, 0)) + both((2, 2)) + items(1, (3, 1)),
+        items(0, (3, 1)) + items(1, (3, 3)),
+        items(0, (3, 3)) + items(1, (3, 2)),
+        items(0, (3, 2)),
+    ]
+
+    def before(n):
+        if n == 1:
+            from_mate(1, 1)
+        if n == 2:
+            hand(1)
+            mates((1, 3), (2, 0))
+        if n == 3:
+            relay(2)
+            spread(3)
+            wo_one()
+            from_mate(1, 2)
+        if n == 4:
+            wo_two()
+            mates((2, 1), (2, 3))
+        if n == 5:
+            hand(2)
+            relay(3)
+            from_mate(3, 0)
+        if n == 6:
+            wo_three()
+            mates((2, 2), (3, 1))
+        if n == 7:
+            hand(3)
+            wo_swap(1, 2)
+            from_mate(3, 3)
+        if n == 8:
+            wo_swap(3)
+            from_mate(3, 2)
+        if n == 9:
+            close_late()
+
+    slot_v = 0
+    for n, todo in enumerate(plan):
+        before(n)
+        slot_v = run(todo, slot_v, plan[n + 1][0] if n + 1 < len(plan) else None, cold=n == 0)
 
     turned = finish(0)
     for copy in att_last:
@@ -541,13 +568,13 @@
             pltpu.VMEM((4, group, model), BF16),
             pltpu.VMEM((width, heads * rows + 128), F32),
             pltpu.VMEM((4, width, heads * rows), F32),
-            pltpu.VMEM((2, width, 2 * heads * rows), BF16),
+            pltpu.VMEM((2, 2, width, 2 * heads * rows), BF16),
             pltpu.VMEM((n_sp * count, 2 * width), BF16),
-            pltpu.VMEM((3, CHUNK, TILE), F32),
-            pltpu.VMEM((3, 8, TILE), F32),
-            pltpu.VMEM((2, width + ONES, CHUNK), BF16),
-            pltpu.VMEM((2, n_tiles, width + ONES, TILE), F32),
-            pltpu.VMEM((2, n_tiles, 1, TILE), F32),
+            pltpu.VMEM((2, 3, CHUNK, TILE), F32),
+            pltpu.VMEM((2, 3, 8, TILE), F32),
+            pltpu.VMEM((2, 2, width + ONES, CHUNK), BF16),
+            pltpu.VMEM((2, 2, n_tiles, width + ONES, TILE), F32),
+            pltpu.VMEM((2, 2, n_tiles, 1, TILE), F32),
             pltpu.VMEM((4, rows, group), BF16),
             pltpu.VMEM((3, rows, group), BF16),
             pltpu.VMEM((count, 128), F32),

time: 60.8 us -> 52.1 us (0.86)
  Pallas kernels: 58.7 us -> 49.8 us
    pallas_call x1, Pallas kernels: 58.7 us -> 49.8 us  [body(): pl.pallas_call(kernel, out_shape=(pltpu.VMEM((rows, model), BF16), pltpu....]
where the time goes in v4:
time: 52.1 us; the launch traced here: 51.8 us
  Pallas kernels  49.8 us (96%)
  local copies, waits for them, and re-layouts  1.34 us (3%)
  between operations  0.64 us (1%)
    pallas_call x1, Pallas kernels, body(): pl.pallas_call(kernel, out_shape=(pltpu.VMEM((rows, model), BF16), pltpu....  49.8 us
    unnamed x2, local copies, waits for them, and re-layouts  1.34 us

profile of v4, /device:TPU:1, one launch (start us, length us, event | category | flops | bytes accessed | tf_op | source)
XLA Modules:
  0.0 51.8 jit_solution(11160503096802420361)
XLA Ops:
  0.6 49.8 %attention.1 = (bf16[96,2048]{1,0:T(8,128)(2,1)S(1)}, f32[4,384]{1,0:T(4,128)S(1)}) custom-call(bf16[96,2048]{1,0:T(8,128)(2,1)} %tok_hbm.1, bf16[2048,256]{1,0:T(8,128)(2,1)} %wq_hbm.1, bf16[64,2048]{1,0:T(8,128)(2,1)} %bitcast.2, bf16[64,2048]{1,0:T(8,128)(2,1)} %bitcast.3, bf16[256,2048]{1,0:T(8,128)(2,1)} %wo_hbm.1, bf16[4,64]{1,0:T(4,128)(2,1)} %qg_ref.1, ...), custom_call_target="tpu_custom_call" | custom-call | tf_op jit(solution)/shard_map/attention/pallas_call | solution.py:556
  50.5 0.7 %copy.11 = bf16[96,2048]{1,0:T(8,128)(2,1)} copy(bf16[96,2048]{1,0:T(8,128)(2,1)S(1)} %get-tuple-element.2) | data formatting | bytes 786432
  51.2 0.6 %copy.12 = f32[4,384]{1,0:T(4,128)} copy(f32[4,384]{1,0:T(4,128)S(1)} %get-tuple-element.3) | data formatting | bytes 12288

commit v5 on v4

--- a/solution.py
+++ b/solution.py
@@ -458,12 +458,13 @@
     plan = [
         items(1, (0, 0), (0, 1), (0, 3)),
         both((0, 2)) + items(1, (1, 0)),
-        both((1, 1), (1, 3)),
-        both((2, 0)) + items(1, (1, 2)),
-        items(0, (1, 2)) + both((2, 1)) + items(1, (2, 3)),
-        items(0, (2, 3)) + items(1, (3, 0)),
-        items(0, (3, 0)) + both((2, 2)) + items(1, (3, 1)),
-        items(0, (3, 1)) + items(1, (3, 3)),
+        both((1, 1)),
+        both((1, 3)) + items(1, (2, 0)),
+        items(0, (2, 0)) + both((1, 2)),
+        both((2, 1)) + items(1, (2, 3)),
+        items(0, (2, 3)) + both((3, 0)) + items(1, (3, 1)),
+        items(0, (3, 1)) + items(1, (2, 2)),
+        items(0, (2, 2)) + items(1, (3, 3)),
         items(0, (3, 3)) + items(1, (3, 2)),
         items(0, (3, 2)),
     ]
@@ -472,31 +473,30 @@
         if n == 1:
             from_mate(1, 1)
         if n == 2:
+            spread(3)
             hand(1)
+            wo_one()
             mates((1, 3), (2, 0))
         if n == 3:
             relay(2)
-            spread(3)
-            wo_one()
-            from_mate(1, 2)
         if n == 4:
             wo_two()
-            mates((2, 1), (2, 3))
+            mates((1, 2), (2, 1))
         if n == 5:
+            relay(3)
+            from_mate(2, 3)
+        if n == 6:
             hand(2)
-            relay(3)
-            from_mate(3, 0)
-        if n == 6:
             wo_three()
-            mates((2, 2), (3, 1))
+            mates((3, 0), (3, 1))
         if n == 7:
+            from_mate(2, 2)
+        if n == 8:
             hand(3)
-            wo_swap(1, 2)
             from_mate(3, 3)
-        if n == 8:
-            wo_swap(3)
+        if n == 9:
             from_mate(3, 2)
-        if n == 9:
+        if n == 10:
             close_late()
 
     slot_v = 0
@@ -510,9 +510,7 @@
     keep_logs(0, turned)
     log_ref[...] = jnp.transpose(log_rows[...])[0:heads]
 
-    for block in (1, 2, 3):
-        other = wo_rows(block, 1 - core, 0, 4)
-        send(other, other, wo_send.at[0], wo_recv.at[block, 3], to_mate).wait_recv()
+    wo_swap(1, 2, 3)
 
     cols = 512
 
@@ -522,23 +520,26 @@
     def times(x, block, n):
         return jnp.dot(x, wo[block, :, columns(n)], preferred_element_type=F32)
 
-    att_late[0].wait_recv()
     for n in range(model // cols):
-        product[:, columns(n)] = times(att[0], 0, n) + times(att_in[2], 3, n)
-    for copy in att_late[1:] + att_last:
-        copy.wait_recv()
-    for n in range(model // cols):
-        total = product[:, columns(n)] + times(att_in[0], 1, n) + times(att_in[1], 2, n)
-        mixed_ref[:, columns(n)] = total.astype(BF16)
-
-    for copy in token_out + token_on + wo_out + wo_on + att_late + att_last:
+        product[:, columns(n)] = times(att[0], 0, n)
+    for copy in token_out + token_on + wo_out + wo_on:
         copy.wait_send()
+    for p in range(4):
+        sent = kv.at[pl.ds(0, 31 * rows)]
+        kv_copy(sent, sent, p, 0, core, to_mate).wait_send()
     for block in (1, 2, 3):
         pair_copy(block).wait_send()
         wo_hand(block).wait_send()
-    for p in range(4):
-        sent = kv.at[pl.ds(0, 31 * rows)]
-        kv_copy(sent, sent, p, 0, core, to_mate).wait_send()
+        other = wo_rows(block, 1 - core, 0, 4)
+        send(other, other, wo_send.at[0], wo_recv.at[block, 3], to_mate).wait_recv()
+    for copy in att_late + att_last:
+        copy.wait_send()
+    for copy in att_late + att_last:
+        copy.wait_recv()
+    for n in range(model // cols):
+        total = product[:, columns(n)] + times(att_in[2], 3, n)
+        total = total + times(att_in[0], 1, n) + times(att_in[1], 2, n)
+        mixed_ref[:, columns(n)] = total.astype(BF16)
 
 
 def body(tokens, query_weight, key_weight, value_weight, out_weight, query_gain, key_gain):

time: 52.1 us -> 48.8 us (0.937)
  Pallas kernels: 49.8 us -> 46.7 us
    pallas_call x1, Pallas kernels: 49.8 us -> 46.7 us  [body(): pl.pallas_call(kernel, out_shape=(pltpu.VMEM((rows, model), BF16), pltpu....]
where the time goes in v5:
time: 48.8 us; the launch traced here: 48.7 us
  Pallas kernels  46.7 us (96%)
  local copies, waits for them, and re-layouts  1.34 us (3%)
  between operations  0.64 us (1%)
    pallas_call x1, Pallas kernels, body(): pl.pallas_call(kernel, out_shape=(pltpu.VMEM((rows, model), BF16), pltpu....  46.7 us
    unnamed x2, local copies, waits for them, and re-layouts  1.34 us

profile of v5, /device:TPU:1, one launch (start us, length us, event | category | flops | bytes accessed | tf_op | source)
XLA Modules:
  0.0 48.7 jit_solution(5696278945936206730)
XLA Ops:
  0.6 46.7 %attention.1 = (bf16[96,2048]{1,0:T(8,128)(2,1)S(1)}, f32[4,384]{1,0:T(4,128)S(1)}) custom-call(bf16[96,2048]{1,0:T(8,128)(2,1)} %tok_hbm.1, bf16[2048,256]{1,0:T(8,128)(2,1)} %wq_hbm.1, bf16[64,2048]{1,0:T(8,128)(2,1)} %bitcast.2, bf16[64,2048]{1,0:T(8,128)(2,1)} %bitcast.3, bf16[256,2048]{1,0:T(8,128)(2,1)} %wo_hbm.1, bf16[4,64]{1,0:T(4,128)(2,1)} %qg_ref.1, ...), custom_call_target="tpu_custom_call" | custom-call | tf_op jit(solution)/shard_map/attention/pallas_call | solution.py:557
  47.4 0.7 %copy.11 = bf16[96,2048]{1,0:T(8,128)(2,1)} copy(bf16[96,2048]{1,0:T(8,128)(2,1)S(1)} %get-tuple-element.2) | data formatting | bytes 786432
  48.1 0.6 %copy.12 = f32[4,384]{1,0:T(4,128)} copy(f32[4,384]{1,0:T(4,128)S(1)} %get-tuple-element.3) | data formatting | bytes 12288

commit v6 on v5

--- a/solution.py
+++ b/solution.py
@@ -124,9 +124,10 @@
     for i in range(1, RING):
         pl.semaphore_signal(barrier, inc=1, device_id={"tp": lax.rem(tp + i, RING)}, device_id_type=MESH)
         pl.semaphore_signal(barrier, inc=1, device_id=peer_a(i), device_id_type=MESH)
-        pl.semaphore_signal(barrier, inc=1, device_id=peer_b(i), device_id_type=MESH)
+        if i != 2:
+            pl.semaphore_signal(barrier, inc=1, device_id=peer_b(i), device_id_type=MESH)
     pl.semaphore_signal(barrier, inc=1, device_id={"sp": mate}, device_id_type=MESH)
-    pl.semaphore_wait(barrier, 3 * (RING - 1) + 1)
+    pl.semaphore_wait(barrier, 3 * (RING - 1))
 
     def send(src, dst, send_sem, recv_sem, where):
         return pltpu.make_async_remote_copy(
@@ -287,9 +288,9 @@
         spot = wo_rows(block, core, 2 * parity, 2)
         return send(spot, spot, wo_send.at[5 + block], wo_recv.at[block, 2], to_pair)
 
-    def wo_hand(block):
-        spot = wo_rows(block, core, 0, 4)
-        return send(spot, spot, wo_send.at[8 + block], wo_recv.at[block, 3], to_mate)
+    def wo_hand(block, mine):
+        spot = wo_rows(block, core, 2 * parity if mine else 2 - 2 * parity, 2)
+        return send(spot, spot, wo_send.at[(8 if mine else 11) + block], wo_recv.at[block, 3], to_mate)
 
     def piece_work(p):
         make_kv(p)
@@ -311,8 +312,6 @@
     for copy in wo_out:
         copy.start()
     piece_work(1)
-    relay(0)
-    from_mate(0, 0)
 
     def turn(chunk, slot):
         at = pl.ds(pl.multiple_of(chunk * CHUNK, CHUNK), CHUNK)
@@ -380,16 +379,19 @@
         for copy, block in zip(wo_rest, (1, 2)):
             copy.wait_recv()
             pair_copy(block).start()
+            wo_hand(block, True).start()
 
     def wo_three():
         for copy in wo_on:
             copy.wait_recv()
         pair_copy(3).start()
+        wo_hand(3, True).start()
 
     def wo_swap(*blocks):
         for block in blocks:
-            pair_copy(block).wait_recv()
-            wo_hand(block).start()
+            spot = wo_rows(block, core, 2 - 2 * parity, 2)
+            send(spot, spot, wo_send.at[0], wo_recv.at[block, 2], to_pair).wait_recv()
+            wo_hand(block, False).start()
 
     def close_late():
         keep_logs(1, finish(1))
@@ -444,10 +446,13 @@
         for spot in spots:
             from_mate(*spot)
 
+    from_mate(0, 0)
+    run(items(0, (0, 0)), 0, cold=True)
+    relay(0)
     next_piece(2)
     spread(1)
     mates((0, 1), (0, 3))
-    run(items(0, (0, 0), (0, 1), (0, 3)), 0, cold=True)
+    run(items(0, (0, 1), (0, 3)), 0, cold=True)
     hand(0)
     from_mate(1, 0)
     run(items(0, (1, 0)), 0, cold=True)
@@ -465,8 +470,8 @@
         items(0, (2, 3)) + both((3, 0)) + items(1, (3, 1)),
         items(0, (3, 1)) + items(1, (2, 2)),
         items(0, (2, 2)) + items(1, (3, 3)),
-        items(0, (3, 3)) + items(1, (3, 2)),
-        items(0, (3, 2)),
+        items(1, (3, 2)),
+        items(0, (3, 3), (3, 2)),
     ]
 
     def before(n):
@@ -479,15 +484,15 @@
             mates((1, 3), (2, 0))
         if n == 3:
             relay(2)
+            wo_two()
         if n == 4:
-            wo_two()
             mates((1, 2), (2, 1))
         if n == 5:
             relay(3)
+            wo_three()
             from_mate(2, 3)
         if n == 6:
             hand(2)
-            wo_three()
             mates((3, 0), (3, 1))
         if n == 7:
             from_mate(2, 2)
@@ -498,11 +503,13 @@
             from_mate(3, 2)
         if n == 10:
             close_late()
+            wo_swap(1, 2)
 
     slot_v = 0
     for n, todo in enumerate(plan):
         before(n)
-        slot_v = run(todo, slot_v, plan[n + 1][0] if n + 1 < len(plan) else None, cold=n == 0)
+        ahead = plan[n + 1][0] if n + 1 < len(plan) and n != 8 else None
+        slot_v = run(todo, slot_v, ahead, cold=n in (0, 9))
 
     turned = finish(0)
     for copy in att_last:
@@ -510,7 +517,7 @@
     keep_logs(0, turned)
     log_ref[...] = jnp.transpose(log_rows[...])[0:heads]
 
-    wo_swap(1, 2, 3)
+    wo_swap(3)
 
     cols = 512
 
@@ -529,16 +536,19 @@
         kv_copy(sent, sent, p, 0, core, to_mate).wait_send()
     for block in (1, 2, 3):
         pair_copy(block).wait_send()
-        wo_hand(block).wait_send()
+        wo_hand(block, True).wait_send()
+        wo_hand(block, False).wait_send()
         other = wo_rows(block, 1 - core, 0, 4)
         send(other, other, wo_send.at[0], wo_recv.at[block, 3], to_mate).wait_recv()
     for copy in att_late + att_last:
         copy.wait_send()
-    for copy in att_late + att_last:
+    for copy in att_late[1:] + att_last:
         copy.wait_recv()
     for n in range(model // cols):
+        product[:, columns(n)] += times(att_in[0], 1, n) + times(att_in[1], 2, n)
+    att_late[0].wait_recv()
+    for n in range(model // cols):
         total = product[:, columns(n)] + times(att_in[2], 3, n)
-        total = total + times(att_in[0], 1, n) + times(att_in[1], 2, n)
         mixed_ref[:, columns(n)] = total.astype(BF16)
 
 
@@ -585,7 +595,7 @@
             dma((4, 2)),
             dma((4,)),
             dma((4, RING, 2)),
-            dma((12,)),
+            dma((15,)),
             dma((4, 4)),
             dma((5,)),
             dma((3, 2)),

time: 48.8 us -> 48.3 us (0.990)
  Pallas kernels: 46.7 us -> 46.1 us
    pallas_call x1, Pallas kernels: 46.7 us -> 46.1 us  [body(): pl.pallas_call(kernel, out_shape=(pltpu.VMEM((rows, model), BF16), pltpu....]
where the time goes in v6:
time: 48.3 us; the launch traced here: 48.1 us
  Pallas kernels  46.1 us (95%)
  local copies, waits for them, and re-layouts  1.34 us (3%)
  between operations  0.64 us (1%)
    pallas_call x1, Pallas kernels, body(): pl.pallas_call(kernel, out_shape=(pltpu.VMEM((rows, model), BF16), pltpu....  46.1 us
    unnamed x2, local copies, waits for them, and re-layouts  1.34 us

profile of v6, /device:TPU:1, one launch (start us, length us, event | category | flops | bytes accessed | tf_op | source)
XLA Modules:
  0.0 48.1 jit_solution(7110333568082975641)
XLA Ops:
  0.6 46.1 %attention.1 = (bf16[96,2048]{1,0:T(8,128)(2,1)S(1)}, f32[4,384]{1,0:T(4,128)S(1)}) custom-call(bf16[96,2048]{1,0:T(8,128)(2,1)} %tok_hbm.1, bf16[2048,256]{1,0:T(8,128)(2,1)} %wq_hbm.1, bf16[64,2048]{1,0:T(8,128)(2,1)} %bitcast.2, bf16[64,2048]{1,0:T(8,128)(2,1)} %bitcast.3, bf16[256,2048]{1,0:T(8,128)(2,1)} %wo_hbm.1, bf16[4,64]{1,0:T(4,128)(2,1)} %qg_ref.1, ...), custom_call_target="tpu_custom_call" | custom-call | tf_op jit(solution)/shard_map/attention/pallas_call | solution.py:567
  46.8 0.7 %copy.11 = bf16[96,2048]{1,0:T(8,128)(2,1)} copy(bf16[96,2048]{1,0:T(8,128)(2,1)S(1)} %get-tuple-element.2) | data formatting | bytes 786432
  47.5 0.6 %copy.12 = f32[4,384]{1,0:T(4,128)} copy(f32[4,384]{1,0:T(4,128)S(1)} %get-tuple-element.3) | data formatting | bytes 12288
